TPU v7x, 32 devices: a whole 2x2x4 slice. The times are simulated.
32 devices in a mesh: ep: 8 (over z, core), tp: 4 (over y, x).
Axes of the slice: x: 2, y: 2, z: 4, core: 2. Of those that a mesh axis runs over, the one named last changes fastest.
Arguments:
- tokens: bfloat16 [128, 2048], P('ep'), may hold values from -6 to 6
- mix_gain: float32 [2048], replicated, may hold values from 0.1 to 1.9
- gate_weight: bfloat16 [2048, 1024], P('ep', 'tp'), may hold values from -0.125 to 0.125
- inner_weight: bfloat16 [2048, 1024], P('ep', 'tp'), may hold values from -0.125 to 0.125
- write_weight: bfloat16 [2048, 512], P('ep'), may hold values from -0.125 to 0.125
- read_weight: bfloat16 [2048, 512], P('ep'), may hold values from -0.125 to 0.125
- step_weight: bfloat16 [2048, 16], P('ep'), may hold values from -0.125 to 0.125
- step_bias: float32 [16], replicated, may hold values from -2 to 1
- decay_log: float32 [16], replicated, may hold values from -1 to 1.5
- skip_scale: float32 [16], replicated, may hold values from 0.5 to 2
- inner_taps: bfloat16 [4, 1024], P(None, 'tp'), may hold values from -3 to 3
- access_taps: bfloat16 [2, 4, 512], replicated, may hold values from -3 to 3
- inner_history: bfloat16 [128, 3, 1024], P('ep', None, 'tp'), may hold values from -6 to 6
- access_history: bfloat16 [128, 2, 3, 512], P('ep'), may hold values from -6 to 6
- recurrent: float32 [128, 16, 64, 128], P('ep', 'tp'), may hold values from -3 to 3
- head_gain: float32 [1024], P('tp'), may hold values from 0.1 to 1.9
- mixer_out: bfloat16 [1024, 2048], P('tp'), may hold values from -0.1875 to 0.1875
- moe_gain: float32 [2048], replicated, may hold values from 0.1 to 1.9
- expert_ids: int32 [128, 2], P('ep'), may hold values from 0 to 7, all different within a row; in each aligned block of 16 rows (0 to 15, 16 to 31, ...) at most 8 rows name the same one
- route_scores: float32 [128, 2], P('ep'), may hold values from -6 to 6
- expert_gate: bfloat16 [8, 2048, 4096], P('ep', None, 'tp'), may hold values from -0.125 to 0.125
- expert_up: bfloat16 [8, 2048, 4096], P('ep', None, 'tp'), may hold values from -0.125 to 0.125
- expert_down: bfloat16 [8, 4096, 2048], P('ep', 'tp'), may hold values from -0.1875 to 0.1875
- blend_vector: bfloat16 [2048], replicated, may hold values from -0.125 to 0.125
- dense_gate: bfloat16 [2048, 7168], P('tp', 'ep'), may hold values from -0.125 to 0.125
- dense_up: bfloat16 [2048, 7168], P('tp', 'ep'), may hold values from -0.125 to 0.125
- dense_down: bfloat16 [7168, 2048], P('ep', 'tp'), may hold values from -0.125 to 0.125
Outputs:
- output: float32 [128, 2048], P('ep', 'tp')
- new_recurrent: float32 [128, 16, 64, 128], P('ep', 'tp')
- new_inner_history: bfloat16 [128, 3, 1024], P('ep', None, 'tp')
- new_access_history: bfloat16 [128, 2, 3, 512], P('ep')
Inputs may be any that keep to these rules, and one draw needn't show every extreme that they name: `expert_ids`: each row names 2 different experts; among the rows of one device no expert is named by more than 8 rows, and in some aligned blocks of 16 rows one expert is named by exactly 8.
All inputs are finite; a program needn't handle non-finite values.
Results may differ from a plain program's by a relative error of at most 0.009.
Values may be sent and summed in bfloat16 or wider, within the bound.
A program may use at most 64 MiB of HBM per device.

v0:
```python
import functools

import jax
import jax.numpy as jnp
from jax import lax
from jax.experimental import pallas as pl
from jax.experimental.pallas import tpu as pltpu
from jax.sharding import PartitionSpec as P

HEADS = 16
HEAD_DIM = 64
GROUPS = 4
STATE = 128
LANES = 128
EPS = 1e-06
BF = jnp.bfloat16
F32 = jnp.float32


def dot(a, b):
    return jnp.dot(a, b, preferred_element_type=F32)


def silu(x):
    return x * (1.0 / (1.0 + jnp.exp(-x)))


def tile_of(extent):
    return 256 if extent % 256 == 0 else extent


def kernel(
    E, T,
    tokens, mix_gain, step_weight, step_bias, decay_log, skip_scale, inner_taps, access_tap,
    inner_past, access_past, head_gain, moe_gain, ids, scores, blend_vector,
    gate_w, inner_w, write_w, read_w, recurrent, mixer_w, eg_w, eu_w, ed_w, dg_w, du_w, dd_w,
    out, new_recurrent, inner_new, maps_all,
    gw, iw, ww, rw, rec, mw, eg, eu, ed, dg, du, dd,
    xs, xr, ps, pr, ms, mr, rbuf, hbuf, cbuf, gacc, uacc, actb, dps, dpr, dab, es, er, own, fs, fr, nrec,
    load_sem, s_ep, r_ep, s_tp, r_tp, s_h, r_h, store_sem,
):
    me = lax.axis_index("ep")
    mt = lax.axis_index("tp")
    S, D = tokens.shape
    C = gw.shape[1]
    DC = D // E
    DS = D // T
    U = dg.shape[1]
    FFL = eg.shape[1]
    R = E * S // T
    group = mt * (HEADS // T) // (HEADS // GROUPS)

    cols = pl.ds(pl.multiple_of(group * STATE, STATE), STATE)
    pairs = [
        (gate_w, gw), (inner_w, iw), (write_w.at[:, cols], ww), (read_w.at[:, cols], rw),
        (recurrent, rec), (mixer_w, mw), (dg_w, dg), (du_w, du), (eg_w, eg), (eu_w, eu),
        (dd_w, dd), (ed_w, ed),
    ]
    loads = [pltpu.make_async_copy(a, b, load_sem.at[i]) for i, (a, b) in enumerate(pairs)]
    for c in loads:
        c.start()

    barrier = pltpu.get_barrier_semaphore()
    for k in range(1, E):
        pl.semaphore_signal(barrier, inc=1, device_id={"ep": lax.rem(me + k, E)},
                            device_id_type=pl.DeviceIdType.MESH)
    for k in range(1, T):
        pl.semaphore_signal(barrier, inc=1, device_id={"tp": lax.rem(mt + k, T)},
                            device_id_type=pl.DeviceIdType.MESH)

    sends = []

    def remote(src, dst, send, recv, axis, target):
        c = pltpu.make_async_remote_copy(
            src_ref=src, dst_ref=dst, send_sem=send, recv_sem=recv,
            device_id={axis: target}, device_id_type=pl.DeviceIdType.MESH)
        c.start()
        sends.append(c)
        return c

    def ep_send(phase, src_of, dst):
        got = []
        for k in range(1, E):
            to = lax.rem(me + k, E)
            got.append(remote(src_of(to), dst, s_ep.at[phase, k], r_ep.at[phase, k], "ep", to))
        return got

    def tp_send(phase, src_of, dst):
        got = []
        for k in range(1, T):
            to = lax.rem(mt + k, T)
            got.append(remote(src_of(to), dst, s_tp.at[phase, k], r_tp.at[phase, k], "tp", to))
        return got

    def arrive(copies):
        for c in copies:
            c.wait_recv()

    tok = tokens[...].astype(F32)
    scale = lax.rsqrt(jnp.mean(tok * tok, axis=-1, keepdims=True) + EPS)
    normed = (tok * scale * mix_gain[...]).astype(BF)
    for j in range(E):
        xs[j] = normed[:, j * DC:(j + 1) * DC]
    xr[me] = xs[me]
    pl.semaphore_wait(barrier, (E - 1) + (T - 1))
    got = ep_send(0, lambda to: xs.at[to], xr.at[me])

    lane = lax.broadcasted_iota(jnp.int32, (S, LANES), 1)
    diagonal = lax.broadcasted_iota(jnp.int32, (S, S), 0) == lax.broadcasted_iota(jnp.int32, (S, S), 1)

    def column(row):
        return jnp.sum(jnp.where(diagonal, row, 0.0), axis=-1, keepdims=True)

    lane_f = lane.astype(F32)
    names = ids[...].astype(F32)
    ranks = scores[...]
    first = 1.0 / (1.0 + jnp.exp(column(ranks[1:2]) - column(ranks[0:1])))
    combine = jnp.where(lane_f == column(names[0:1]), first, 0.0) + jnp.where(
        lane_f == column(names[1:2]), 1.0 - first, 0.0)

    for c in loads[:4]:
        c.wait()
    arrive(got)

    rows = xr[...].reshape(E * S, DC)
    step_p = lax.dot_general(
        rows, step_weight[...], (((1,), (1,)), ((), ())), preferred_element_type=F32)
    step_hi = step_p.astype(BF)
    step_lo = (step_p - step_hi.astype(F32)).astype(BF)
    M = 2 * STATE
    ps[:, :, 0:STATE] = dot(rows, ww[...]).astype(BF).reshape(E, S, STATE)
    ps[:, :, STATE:M] = dot(rows, rw[...]).astype(BF).reshape(E, S, STATE)
    ps[:, :, M:M + LANES] = jnp.concatenate(
        [step_hi, step_lo, jnp.zeros((E * S, LANES - 2 * HEADS), BF)], axis=1).reshape(E, S, LANES)
    G = M + LANES
    ps[:, :, G:G + C] = dot(rows, gw[...]).astype(BF).reshape(E, S, C)
    ps[:, :, G + C:G + 2 * C] = dot(rows, iw[...]).astype(BF).reshape(E, S, C)
    pr[me] = ps[me]
    got = ep_send(1, lambda to: ps.at[to], pr.at[me])

    chan = lax.broadcasted_iota(jnp.int32, (S, C), 1)
    head_of = mt * (HEADS // T) + chan // HEAD_DIM

    def expand(values):
        total = jnp.zeros((S, C), F32)
        for h in range(HEADS):
            total = jnp.where(head_of == h, values[:, h:h + 1], total)
        return total

    skip = expand(skip_scale[...])
    arrive(got)
    proj = pr[0].astype(F32)
    for j in range(1, E):
        proj = proj + pr[j].astype(F32)
    maps = proj[:, 0:M].astype(BF)
    step_raw = proj[:, M:M + HEADS] + proj[:, M + HEADS:M + 2 * HEADS]
    gate_part = proj[:, G:G + C].astype(BF).astype(F32)
    inner_part = proj[:, G + C:G + 2 * C].astype(BF)
    taps = inner_taps[...].astype(F32)
    conv = inner_part.astype(F32) * taps[3:4]
    for k in range(3):
        conv = conv + inner_past[k].astype(F32) * taps[k:k + 1]
        inner_new[k] = inner_past[k + 1] if k < 2 else inner_part
    mr_maps = maps_all
    ms[:, D:D + M] = maps
    inner = silu(conv)
    access = silu(access_past[...] + maps.astype(F32) * access_tap[...])
    step_x = step_raw + step_bias[...]
    step = jnp.maximum(step_x, 0.0) + jnp.log1p(jnp.exp(-jnp.abs(step_x)))
    decay = jnp.exp(-step * jnp.exp(decay_log[...]))
    push_t = jnp.transpose(expand(step) * inner)
    decay_t = jnp.transpose(expand(decay))
    loads[4].wait()
    seq_lane = lax.broadcasted_iota(jnp.int32, (C, S), 1)
    read_t = jnp.zeros((C, S), F32)
    for t in range(S):
        state = decay_t[:, t:t + 1] * rec[t] + push_t[:, t:t + 1] * access[t:t + 1, 0:STATE]
        nrec[t] = state
        total = jnp.sum(state * access[t:t + 1, STATE:M], axis=-1, keepdims=True)
        read_t = jnp.where(seq_lane == t, total, read_t)
    readout = jnp.transpose(read_t) + skip * inner
    gated = readout * silu(gate_part)
    square = gated * gated
    norm = jnp.zeros((S, C), F32)
    for h in range(C // HEAD_DIM):
        here = chan // HEAD_DIM == h
        mean = jnp.sum(jnp.where(here, square, 0.0), axis=-1, keepdims=True) / HEAD_DIM
        norm = jnp.where(here, lax.rsqrt(mean + EPS), norm)
    head_out = (gated * norm * head_gain[...]).astype(BF)
    loads[5].wait()
    for j in range(T):
        ms[:, j * DS:(j + 1) * DS] = dot(head_out, mw[:, j * DS:(j + 1) * DS]).astype(BF)
    mr[mt] = ms[...]
    got = tp_send(0, lambda to: ms, mr.at[mt])
    store = pltpu.make_async_copy(nrec, new_recurrent, store_sem.at[0])
    store.start()
    arrive(got)
    mixed = mr[0].astype(F32)
    for j in range(1, T):
        mixed = mixed + mr[j].astype(F32)
    mr_maps[...] = mr[:, :, D:D + M]
    resid = tok + mixed[:, 0:D].astype(BF).astype(F32)
    scale = lax.rsqrt(jnp.mean(resid * resid, axis=-1, keepdims=True) + EPS)
    hidden = (resid * scale * moe_gain[...]).astype(BF)
    for q in range(T):
        rbuf[q] = resid[:, q * DS:(q + 1) * DS]
        hbuf[q, me] = hidden[:, q * DS:(q + 1) * DS]
    scorer = blend_vector[...].astype(F32)
    blend = jnp.zeros((S, LANES), F32)
    for j in range(D // LANES):
        blend = blend + hidden[:, j * LANES:(j + 1) * LANES].astype(F32) * scorer[j:j + 1]
    blend = jnp.sum(blend, axis=-1, keepdims=True)
    blend = 1.0 / (1.0 + jnp.exp(-blend))
    cbuf[me] = jnp.where(lane == E, blend, combine)

    twin = me + 1 - 2 * lax.rem(me, 2)
    chips = E // 2
    pieces = []
    for j in range(T):
        q = lax.rem(mt + j, T)
        here = []
        for m in range(1, chips):
            to = lax.rem(me + 2 * m, E)
            here.append(remote(hbuf.at[q, me], hbuf.at[q, me], s_h.at[j, 2 * m], r_h.at[j, 2 * m], "ep", to))
        beside = remote(hbuf.at[q, me], hbuf.at[q, me], s_h.at[j, 1], r_h.at[j, 1], "ep", twin)
        pieces.append((here, beside))
        if j == 0:
            got_c = ep_send(2, lambda to: cbuf.at[me], cbuf.at[me])

    def relay(j):
        q = lax.rem(mt + j, T)
        here, beside = pieces[j]
        passed = [beside]
        for m in range(1, chips):
            here[m - 1].wait_recv()
            source = lax.rem(me + E - 2 * m, E)
            block = hbuf.at[q, source]
            passed.append(remote(block, block, s_h.at[j, 2 * m + 1], r_h.at[j, 2 * m + 1], "ep", twin))
        return passed

    passed = relay(0)
    got_d = None
    tile = tile_of(FFL)
    for c in loads[6:10]:
        c.wait()
    for j in range(T):
        q = lax.rem(mt + j, T)
        arrive(passed)
        here = hbuf[q].reshape(E * S, DS)
        if j == 0:
            dps[:, 0] = dot(here, dg[...]).astype(BF).reshape(T, R, U)
            dps[:, 1] = dot(here, du[...]).astype(BF).reshape(T, R, U)
            dpr[mt] = dps[mt]
            got_d = tp_send(1, lambda to: dps.at[to], dpr.at[mt])
        if j < T - 1:
            passed = relay(j + 1)
        rows_q = pl.ds(pl.multiple_of(q * DS, DS), DS)

        @pl.loop(0, FFL // tile)
        def _(n, here=here, rows_q=rows_q, j=j):
            at = pl.ds(pl.multiple_of(n * tile, tile), tile)
            g = dot(here, eg[rows_q, at])
            u = dot(here, eu[rows_q, at])
            if j > 0:
                g = g + gacc[:, at]
                u = u + uacc[:, at]
            if j < T - 1:
                gacc[:, at] = g
                uacc[:, at] = u
            else:
                actb[:, at] = (silu(g) * u).astype(BF)

    arrive(got_d)
    dsum = dpr[0].astype(F32)
    for j in range(1, T):
        dsum = dsum + dpr[j].astype(F32)
    dab[mt] = (silu(dsum[0]) * dsum[1]).astype(BF)
    got_a = tp_send(2, lambda to: dab.at[mt], dab.at[mt])

    arrive(got_c)
    weights = cbuf[...].reshape(E * S, LANES)
    wide = lax.broadcasted_iota(jnp.int32, (E * S, LANES), 1)
    mine = jnp.sum(jnp.where(wide == me, weights, 0.0), axis=-1, keepdims=True)
    blends = jnp.sum(jnp.where(wide == E, weights, 0.0), axis=-1, keepdims=True)
    loads[10].wait()
    loads[11].wait()
    got_e = []
    dtile = tile_of(DS)
    for k in range(1, T + 1):
        to = lax.rem(mt + k, T)

        @pl.loop(0, DS // dtile)
        def _(n, to=to, k=k):
            base = pl.multiple_of(n * dtile, dtile)
            at = pl.ds(pl.multiple_of(to * DS + n * dtile, dtile), dtile)
            share = dot(actb[...], ed[:, at]) * mine
            if k < T:
                es[k, :, pl.ds(base, dtile)] = share.astype(BF)
            else:
                own[:, pl.ds(base, dtile)] = share

        if k < T:
            got_e.append(remote(es.at[k], er.at[k], s_tp.at[3, k], r_tp.at[3, k], "tp", to))
    arrive(got_a)
    total = own[...] + blends * dot(dab[...].reshape(E * S, U), dd[...])
    arrive(got_e)
    for k in range(1, T):
        total = total + er[k].astype(F32)
    fs[...] = total.astype(BF).reshape(E, S, DS)
    own[...] = total
    fr[me] = jnp.zeros((S, DS), BF)
    got = ep_send(3, lambda to: fs.at[to], fr.at[me])
    final = rbuf[mt] + own[pl.ds(pl.multiple_of(me * S, S), S), :]
    arrive(got)
    for j in range(E):
        final = final + fr[j].astype(F32)
    out[...] = final
    store.wait()
    for c in sends:
        c.wait_send()


def local(
    E, T,
    tokens, mix_gain, gate_weight, inner_weight, write_weight, read_weight, step_weight, step_bias,
    decay_log, skip_scale, inner_taps, access_taps, inner_history, access_history, recurrent,
    head_gain, mixer_out, moe_gain, expert_ids, route_scores, expert_gate, expert_up, expert_down,
    blend_vector, dense_gate, dense_up, dense_down,
):
    S, D = tokens.shape
    C = gate_weight.shape[1]
    DC, DS = D // E, D // T
    U = dense_gate.shape[1]
    FFL = expert_gate.shape[2]
    rows = E * S
    R = rows // T
    M = 2 * STATE
    PW = M + LANES + 2 * C
    group = lax.axis_index("tp") * (HEADS // T) // (HEADS // GROUPS)
    hist = lax.dynamic_slice_in_dim(access_history, group * STATE, STATE, 3)
    taps = lax.dynamic_slice_in_dim(access_taps, group * STATE, STATE, 2).astype(F32)
    access_past = jnp.sum(hist.astype(F32) * taps[None, :, :3], axis=2).reshape(S, M)
    vmem = pl.BlockSpec(memory_space=pltpu.VMEM)
    hbm = pl.BlockSpec(memory_space=pl.ANY)
    V = pltpu.VMEM
    DMA = pltpu.SemaphoreType.DMA
    out, new_recurrent, inner_new, maps_all = pl.pallas_call(
        functools.partial(kernel, E, T),
        name="decode_step",
        out_shape=(
            jax.ShapeDtypeStruct((S, DS), F32),
            jax.ShapeDtypeStruct((S, C, STATE), F32),
            jax.ShapeDtypeStruct((3, S, C), BF),
            jax.ShapeDtypeStruct((T, S, M), BF),
        ),
        in_specs=[vmem] * 15 + [hbm] * 12,
        out_specs=(vmem, hbm, vmem, vmem),
        scratch_shapes=[
            V((DC, C), BF), V((DC, C), BF), V((DC, STATE), BF), V((DC, STATE), BF),
            V((S, C, STATE), F32), V((C, D), BF),
            V((D, FFL), BF), V((D, FFL), BF), V((FFL, D), BF),
            V((DS, U), BF), V((DS, U), BF), V((U, DS), BF),
            V((E, S, DC), BF), V((E, S, DC), BF), V((E, S, PW), BF), V((E, S, PW), BF),
            V((S, D + M), BF), V((T, S, D + M), BF), V((T, S, DS), F32), V((T, E, S, DS), BF),
            V((E, S, LANES), F32), V((rows, FFL), F32), V((rows, FFL), F32), V((rows, FFL), BF),
            V((T, 2, R, U), BF), V((T, 2, R, U), BF), V((T, R, U), BF),
            V((T, rows, DS), BF), V((T, rows, DS), BF), V((rows, DS), F32),
            V((E, S, DS), BF), V((E, S, DS), BF), V((S, C, STATE), F32),
            DMA((12,)), DMA((4, E)), DMA((4, E)), DMA((4, T)), DMA((4, T)),
            DMA((T, E)), DMA((T, E)), DMA((1,)),
        ],
        compiler_params=pltpu.CompilerParams(
            collective_id=0, has_side_effects=True, vmem_limit_bytes=60 * 1024 * 1024
        ),
    )(
        tokens, mix_gain[None], step_weight.T, step_bias[None], decay_log[None], skip_scale[None],
        inner_taps, taps[:, 3].reshape(1, M), inner_history.transpose(1, 0, 2), access_past,
        head_gain[None], moe_gain[None], expert_ids.T, route_scores.T, blend_vector.reshape(-1, LANES),
        gate_weight, inner_weight, write_weight, read_weight,
        recurrent.reshape(S, C, STATE), mixer_out,
        expert_gate[0], expert_up[0], expert_down[0], dense_gate, dense_up, dense_down,
    )
    new_inner = inner_new.transpose(1, 0, 2)
    maps = maps_all[:: max(1, T // GROUPS)].reshape(-1, S, 2, STATE)
    maps = maps.transpose(1, 2, 0, 3).reshape(S, 2, 1, GROUPS * STATE)
    new_access = jnp.concatenate([access_history[:, :, 1:], maps], axis=2)
    return out, new_recurrent.reshape(recurrent.shape), new_inner, new_access


def solution(mesh):
    in_specs = (
        P("ep", None), P(), P("ep", "tp"), P("ep", "tp"), P("ep", None), P("ep", None),
        P("ep", None), P(), P(), P(), P(None, "tp"), P(), P("ep", None, "tp"),
        P("ep", None, None, None), P("ep", "tp", None, None), P("tp"), P("tp", None), P(),
        P("ep", None), P("ep", None), P("ep", None, "tp"), P("ep", None, "tp"),
        P("ep", "tp", None), P(), P("tp", "ep"), P("tp", "ep"), P("ep", "tp"),
    )
    out_specs = (
        P("ep", "tp"), P("ep", "tp", None, None), P("ep", None, "tp"), P("ep", None, None, None),
    )
    body = functools.partial(local, mesh.shape["ep"], mesh.shape["tp"])
    return jax.shard_map(body, mesh=mesh, in_specs=in_specs, out_specs=out_specs, check_vma=False)
```

profile of v0, /device:TPU:0, one launch (start us, length us, event | category | flops | bytes accessed | tf_op | source)
XLA Modules:
  0.0 65.5 jit_solution(17790960401161661149)
XLA Ops:
  0.7 0.7 %dynamic-slice_convert_fusion = f32[2,4,128]{2,1,0:T(4,128)S(1)} fusion(bf16[2,4,512]{2,1,0:T(4,128)(2,1)} %param.38, s32[]{:T(128)S(6)} %select_n.10), kind=kLoop, calls=%fused_computation.3 | loop fusion | flops 1024 | bytes 6148 | tf_op jit(solution)/shard_map/convert_element_type | solution.py:341
  1.3 0.8 %multiply_reduce_fusion = f32[16,2,128]{2,1,0:T(2,128)S(1)} fusion(f32[2,3,128]{2,0,1:T(2,128)S(1)} %copy.31, bf16[16,2,3,512]{3,1,2,0:T(2,128)(2,1)} %param.40, s32[]{:T(128)S(6)} %select_n.10), kind=kLoop, calls=%fused_computation.1 | loop fusion | flops 32768 | bytes 44036 | tf_op jit(solution)/shard_map/reduce_sum | solution.py:342
  2.1 0.6 copy.35
  2.7 0.6 slice_bitcast_fusion.access_tap
  3.3 0.0 slice-start
  3.3 55.4 %decode_step.1 = (f32[16,512]{1,0:T(8,128)}, f32[16,256,128]{2,1,0:T(8,128)}, bf16[3,16,256]{2,1,0:T(8,128)(2,1)}, bf16[4,16,256]{2,1,0:T(8,128)(2,1)}) custom-call(bf16[16,2048]{1,0:T(8,128)(2,1)} %tokens.1, f32[1,2048]{1,0:T(1,128)} %bitcast.36, bf16[16,256]{1,0:T(8,128)(2,1)} %bitcast.37, f32[1,16]{1,0:T(1,128)} %bitcast.43, f32[1,16]{1,0:T(1,128)} %bitcast.44, ...), custom_call_target="tpu_custom_call" | custom-call | tf_op jit(solution)/shard_map/decode_step/pallas_call | solution.py:347
  58.7 0.0 copy-start
  58.7 0.8 %reshape.31 = bf16[4,16,2,128]{3,2,1,0:T(2,128)(2,1)S(1)} reshape(bf16[4,16,256]{2,1,0:T(8,128)(2,1)} %get-tuple-element.11) | data formatting | bytes 65536 | tf_op jit(solution)/shard_map/reshape | solution.py:384
  59.5 0.0 slice-done
  59.6 0.8 %pad_maximum_fusion = bf16[16,2,3,512]{3,1,2,0:T(2,128)(2,1)} fusion(bf16[16,2,1,512]{3,1,2,0:T(2,128)(2,1)S(1)} %reshape.32, bf16[16,2,2,512]{3,1,2,0:T(2,128)(2,1)S(1)} %slice-done), kind=kLoop, calls=%fused_computation | loop fusion | flops 49152 | bytes 196608 | tf_op jit(solution)/shard_map/concatenate | solution.py:386
  60.3 1.4 %copy.39 = f32[16,512]{1,0:T(8,128)} copy(f32[16,512]{1,0:T(8,128)} %get-tuple-element.16) | data formatting | bytes 65536
  61.7 3.2 %copy.40 = f32[16,4,64,128]{3,2,1,0:T(8,128)} copy(f32[16,4,64,128]{3,2,1,0:T(8,128)} %bitcast.28) | data formatting | bytes 4194304
  64.9 0.0 copy-done
  64.9 0.6 copy.41
  (3 shorter events, 0.0 us)
Async XLA Ops:
  3.3 56.2 %slice-start = ((bf16[16,2,3,512]{3,1,2,0:T(2,128)(2,1)}), bf16[16,2,2,512]{3,1,2,0:T(2,128)(2,1)S(1)}, s32[]{:S(2)}) async-start(bf16[16,2,3,512]{3,1,2,0:T(2,128)(2,1)} %param.40), calls=%async_computation | async-start | bytes 131072 | tf_op jit(solution)/shard_map/slice | solution.py:386
  58.7 6.2 %copy-start = (bf16[3,16,256]{2,1,0:T(8,128)(2,1)S(1)}, bf16[3,16,256]{2,1,0:T(8,128)(2,1)}, u32[]{:S(2)}) copy-start(bf16[3,16,256]{2,1,0:T(8,128)(2,1)} %get-tuple-element.10) | copy-start | bytes 73732
where the time goes:
time: 65.9 us; the launch traced here: 65.5 us
  Pallas kernels  55.4 us (84%)
  local copies, waits for them, and re-layouts  7.14 us (11%)
  other arithmetic  2.24 us (3%)
  between operations  0.69 us (1%)
    pallas_call x1, Pallas kernels, local(): pl.pallas_call(functools.partial(kernel, E, T), name='decode_step', out_s...  55.4 us
    unnamed x6, local copies, waits for them, and re-layouts  5.75 us

commit v1 on v0

v1 whole, which is shorter than its diff:
```python
import functools

import jax
import jax.numpy as jnp
from jax import lax
from jax.experimental import pallas as pl
from jax.experimental.pallas import tpu as pltpu
from jax.sharding import PartitionSpec as P

HEADS = 16
HEAD_DIM = 64
GROUPS = 4
STATE = 128
LANES = 128
TOP = 2
EPS = 1e-06
BF = jnp.bfloat16
F32 = jnp.float32


def dot(a, b):
    return jnp.dot(a, b, preferred_element_type=F32)


def silu(x):
    return x * (1.0 / (1.0 + jnp.exp(-x)))


def tile_of(extent):
    return 256 if extent % 256 == 0 else extent


def kernel(
    E, T, CAP,
    tokens_h, mix_gain_h, step_weight_h, step_bias_h, decay_log_h, skip_scale_h, inner_taps_h, access_taps_h,
    inner_past_h, access_past_h, head_gain_h, moe_gain_h, ids_h, scores_h, blend_vector_h,
    gate_w, inner_w, write_w, read_w, recurrent, mixer_w, eg_w, eu_w, ed_w, dg_w, du_w, dd_w,
    out, nrec, inner_new, access_new,
    tokens, mix_gain, step_weight, step_bias, decay_log, skip_scale, inner_taps, access_taps,
    inner_past, access_past, head_gain, moe_gain, ids, scores, blend_vector,
    gw, iw, ww, rw, rec, mw, eg, eu, ed, dg, du, dd,
    xs, xr, ps, pr, pg, pgr, rcat, ms, mr, mm, mmr, rbuf, hbuf, sel, gacc, uacc, actb, dps, dpr, dab, es, er, fs, fr,
    small_sem, load_sem, s_ep, r_ep, s_tp, r_tp, s_h, r_h, s_x, r_x,
):
    me = lax.axis_index("ep")
    mt = lax.axis_index("tp")
    S, D = tokens.shape
    C = gw.shape[1]
    DC = D // E
    DS = D // T
    U = dg.shape[1]
    FFL = eg.shape[1]
    R = E * S // T
    N = E * CAP
    M = 2 * STATE
    group = mt * (HEADS // T) // (HEADS // GROUPS)

    barrier = pltpu.get_barrier_semaphore()
    for k in range(1, E):
        pl.semaphore_signal(barrier, inc=1, device_id={"ep": lax.rem(me + k, E)},
                            device_id_type=pl.DeviceIdType.MESH)
    for k in range(1, T):
        pl.semaphore_signal(barrier, inc=1, device_id={"tp": lax.rem(mt + k, T)},
                            device_id_type=pl.DeviceIdType.MESH)

    cols = pl.ds(pl.multiple_of(group * STATE, STATE), STATE)
    small = [
        (tokens_h, tokens), (mix_gain_h, mix_gain), (ids_h, ids), (step_weight_h, step_weight),
        (scores_h, scores), (step_bias_h, step_bias), (decay_log_h, decay_log), (skip_scale_h, skip_scale),
        (inner_taps_h, inner_taps), (access_taps_h.at[:, :, cols], access_taps), (inner_past_h, inner_past),
        (access_past_h.at[:, :, :, cols], access_past), (head_gain_h, head_gain), (moe_gain_h, moe_gain),
        (blend_vector_h, blend_vector), (access_past_h.at[:, 1:3], access_new.at[:, 0:2]),
    ]
    smalls = [pltpu.make_async_copy(a, b, small_sem.at[i]) for i, (a, b) in enumerate(small)]
    pairs = [
        (gate_w, gw), (inner_w, iw), (write_w.at[:, cols], ww), (read_w.at[:, cols], rw),
        (recurrent, rec), (mixer_w, mw), (dg_w, dg), (du_w, du), (eg_w, eg), (eu_w, eu),
        (dd_w, dd), (ed_w, ed),
    ]
    loads = [pltpu.make_async_copy(a, b, load_sem.at[i]) for i, (a, b) in enumerate(pairs)]
    for c in smalls[:4]:
        c.start()
    for c in loads[:4]:
        c.start()
    for c in smalls[4:]:
        c.start()
    for c in loads[4:]:
        c.start()

    sends = []

    def remote(src, dst, send, recv, device):
        c = pltpu.make_async_remote_copy(
            src_ref=src, dst_ref=dst, send_sem=send, recv_sem=recv,
            device_id=device, device_id_type=pl.DeviceIdType.MESH)
        c.start()
        sends.append(c)
        return c

    def ep_send(phase, src_of, dst):
        got = []
        for k in range(1, E):
            to = lax.rem(me + k, E)
            got.append(remote(src_of(to), dst, s_ep.at[phase, k], r_ep.at[phase, k], {"ep": to}))
        return got

    def tp_send(phase, src_of, dst):
        got = []
        for k in range(1, T):
            to = lax.rem(mt + k, T)
            got.append(remote(src_of(to), dst, s_tp.at[phase, k], r_tp.at[phase, k], {"tp": to}))
        return got

    def arrive(copies):
        for c in copies:
            c.wait_recv()

    lane = lax.broadcasted_iota(jnp.int32, (S, LANES), 1)
    lane_f = lane.astype(F32)
    row_i = lax.broadcasted_iota(jnp.int32, (S, S), 0)
    col_i = lax.broadcasted_iota(jnp.int32, (S, S), 1)
    diagonal = row_i == col_i
    earlier = jnp.where(col_i < row_i, 1.0, 0.0)

    def column(row):
        return jnp.sum(jnp.where(diagonal, row, 0.0), axis=-1, keepdims=True)

    for c in smalls[:3]:
        c.wait()
    tok = tokens[...].astype(F32)
    scale = lax.rsqrt(jnp.mean(tok * tok, axis=-1, keepdims=True) + EPS)
    normed = (tok * scale * mix_gain[...]).astype(BF)
    names = ids[...].astype(F32)
    name_a, name_b = column(names[0:1]), column(names[1:2])
    named = jnp.where((lane_f == name_a) | (lane_f == name_b), 1.0, 0.0)
    before = dot(earlier, named)
    rank = jnp.where(named > 0.0, before, -1.0)
    for j in range(E):
        xs[j, :, 0:DC] = normed[:, j * DC:(j + 1) * DC]
        xs[j, :, DC:DC + LANES] = jnp.broadcast_to(rank[:, j:j + 1], (S, LANES)).astype(BF)
    xr[me] = xs[me]
    pl.semaphore_wait(barrier, (E - 1) + (T - 1))
    got = ep_send(0, lambda to: xs.at[to], xr.at[me])

    for c in smalls[3:15]:
        c.wait()
    ranks = scores[...]
    first = 1.0 / (1.0 + jnp.exp(column(ranks[1:2]) - column(ranks[0:1])))
    combine = jnp.where(lane_f == name_a, first, 0.0) + jnp.where(lane_f == name_b, 1.0 - first, 0.0)
    slot = lax.broadcasted_iota(jnp.int32, (S, N), 1)
    slot_rank = lax.rem(slot, CAP).astype(F32)
    mix = jnp.zeros((S, N), F32)
    for e in range(E):
        hit = (slot // CAP == e) & (slot_rank == rank[:, e:e + 1])
        mix = jnp.where(hit, combine[:, e:e + 1], mix)
    mix_hi = mix.astype(BF)
    mix_lo = (mix - mix_hi.astype(F32)).astype(BF)

    taps_k = access_taps[...].astype(F32)
    tap_rows = [jnp.concatenate([taps_k[0, k:k + 1], taps_k[1, k:k + 1]], axis=0) for k in range(4)]
    row_of = lax.broadcasted_iota(jnp.int32, (S, STATE), 0)
    past_w = jnp.zeros((S, STATE), F32)
    past_r = jnp.zeros((S, STATE), F32)
    for s in range(S):
        total = access_past[s, 0].astype(F32) * tap_rows[0]
        for k in range(1, 3):
            total = total + access_past[s, k].astype(F32) * tap_rows[k]
        past_w = jnp.where(row_of == s, total[0:1], past_w)
        past_r = jnp.where(row_of == s, total[1:2], past_r)

    for c in loads[:4]:
        c.wait()
    arrive(got)

    rows = xr[:, :, 0:DC].reshape(E * S, DC)
    step_p = lax.dot_general(
        rows, step_weight[...], (((1,), (1,)), ((), ())), preferred_element_type=F32)
    step_hi = step_p.astype(BF)
    step_lo = (step_p - step_hi.astype(F32)).astype(BF)
    ps[:, :, 0:STATE] = dot(rows, ww[...]).astype(BF).reshape(E, S, STATE)
    ps[:, :, STATE:M] = dot(rows, rw[...]).astype(BF).reshape(E, S, STATE)
    ps[:, :, M:M + LANES] = jnp.concatenate(
        [step_hi, step_lo, jnp.zeros((E * S, LANES - 2 * HEADS), BF)], axis=1).reshape(E, S, LANES)
    G = M + LANES
    ps[:, :, G:G + C] = dot(rows, iw[...]).astype(BF).reshape(E, S, C)
    pr[me] = ps[me]
    got = ep_send(1, lambda to: ps.at[to], pr.at[me])
    pg[...] = dot(rows, gw[...]).astype(BF).reshape(E, S, C)
    pgr[me] = pg[me]
    got_g = ep_send(2, lambda to: pg.at[to], pgr.at[me])

    rank_of = xr[:, :, DC:DC + LANES].reshape(E * S, LANES)[:, 0:N].astype(F32)
    wide = lax.broadcasted_iota(jnp.int32, (E * S, N), 1)
    seq = lax.broadcasted_iota(jnp.int32, (E * S, N), 0)
    chosen = (wide // CAP == seq // S) & (lax.rem(wide, CAP).astype(F32) == rank_of)
    sel[...] = jnp.transpose(jnp.where(chosen, 1.0, 0.0)).astype(BF)

    chan = lax.broadcasted_iota(jnp.int32, (S, C), 1)
    head_of = mt * (HEADS // T) + chan // HEAD_DIM

    def expand(values):
        total = jnp.zeros((S, C), F32)
        for h in range(HEADS):
            total = jnp.where(head_of == h, values[:, h:h + 1], total)
        return total

    skip = expand(skip_scale[...])
    taps = inner_taps[...].astype(F32)
    past = inner_past[0].astype(F32) * taps[0:1]
    for k in range(1, 3):
        past = past + inner_past[k].astype(F32) * taps[k:k + 1]
        inner_new[k - 1] = inner_past[k]
    rate = jnp.exp(decay_log[...])
    loads[4].wait()

    @pl.loop(0, S)
    def _(t):
        value = rec[t]
        high = value.astype(BF)
        rcat[t, :, 0:STATE] = high
        rcat[t, :, STATE:M] = (value - high.astype(F32)).astype(BF)

    arrive(got)
    proj = pr[0].astype(F32)
    for j in range(1, E):
        proj = proj + pr[j].astype(F32)
    maps = proj[:, 0:M].astype(BF)
    step_raw = proj[:, M:M + HEADS] + proj[:, M + HEADS:M + 2 * HEADS]
    inner_part = proj[:, G:G + C].astype(BF)
    inner_new[2] = inner_part
    inner = silu(past + inner_part.astype(F32) * taps[3:4])
    mm[...] = maps
    maps_f = maps.astype(F32)
    write_c = silu(past_w + maps_f[:, 0:STATE] * tap_rows[3][0:1])
    read_c = silu(past_r + maps_f[:, STATE:M] * tap_rows[3][1:2])
    read_hi = read_c.astype(BF).astype(F32)
    read_lo = read_c - read_hi
    spare = LANES - 2 * S
    upper = jnp.concatenate([read_hi, read_lo, jnp.zeros((spare, STATE), F32)], axis=0)
    lower = jnp.concatenate([read_hi, jnp.zeros((spare + S, STATE), F32)], axis=0)
    reader = jnp.concatenate([jnp.transpose(upper), jnp.transpose(lower)], axis=0).astype(BF)
    step_x = step_raw + step_bias[...]
    step = jnp.maximum(step_x, 0.0) + jnp.log1p(jnp.exp(-jnp.abs(step_x)))
    decay = expand(jnp.exp(-step * rate))
    push = expand(step) * inner
    both = jnp.sum(write_c * read_c, axis=-1, keepdims=True)
    seq_lane = lax.rem(lax.broadcasted_iota(jnp.int32, (C, LANES), 1), S)
    read_t = jnp.zeros((C, LANES), F32)
    for t in range(S):
        read_t = jnp.where(seq_lane == t, dot(rcat[t], reader), read_t)
    read_rows = jnp.transpose(read_t)
    recalled = read_rows[0:S] + read_rows[S:2 * S]
    readout = decay * recalled + push * both + skip * inner
    arrive(got_g)
    gate_sum = pgr[0].astype(F32)
    for j in range(1, E):
        gate_sum = gate_sum + pgr[j].astype(F32)
    gated = readout * silu(gate_sum.astype(BF).astype(F32))
    square = gated * gated
    norm = jnp.zeros((S, C), F32)
    for h in range(C // HEAD_DIM):
        here = chan // HEAD_DIM == h
        mean = jnp.sum(jnp.where(here, square, 0.0), axis=-1, keepdims=True) / HEAD_DIM
        norm = jnp.where(here, lax.rsqrt(mean + EPS), norm)
    head_out = (gated * norm * head_gain[...]).astype(BF)
    loads[5].wait()
    for j in range(T):
        ms[:, j * DS:(j + 1) * DS] = dot(head_out, mw[:, j * DS:(j + 1) * DS]).astype(BF)
    mr[mt] = ms[...]
    got = tp_send(0, lambda to: ms, mr.at[mt])
    mmr[mt] = mm[...]
    got_m = tp_send(1, lambda to: mm, mmr.at[mt])

    decay_t = jnp.transpose(decay)
    push_t = jnp.transpose(push)
    for t in range(S):
        nrec[t] = decay_t[:, t:t + 1] * rec[t] + push_t[:, t:t + 1] * write_c[t:t + 1]

    arrive(got)
    mixed = mr[0].astype(F32)
    for j in range(1, T):
        mixed = mixed + mr[j].astype(F32)
    resid = tok + mixed.astype(BF).astype(F32)
    scale = lax.rsqrt(jnp.mean(resid * resid, axis=-1, keepdims=True) + EPS)
    hidden = (resid * scale * moe_gain[...]).astype(BF)
    for q in range(T):
        rbuf[q] = resid[:, q * DS:(q + 1) * DS]
        hbuf[q, me] = hidden[:, q * DS:(q + 1) * DS]

    twin = me + 1 - 2 * lax.rem(me, 2)
    chips = E // 2
    pieces = []
    for j in range(T):
        q = lax.rem(mt + j, T)
        here = []
        for m in range(1, chips):
            to = lax.rem(me + 2 * m, E)
            here.append(remote(hbuf.at[q, me], hbuf.at[q, me], s_h.at[j, 2 * m], r_h.at[j, 2 * m], {"ep": to}))
        beside = remote(hbuf.at[q, me], hbuf.at[q, me], s_h.at[j, 1], r_h.at[j, 1], {"ep": twin})
        pieces.append((here, beside))

    scorer = blend_vector[...].astype(F32)
    blend = jnp.zeros((S, LANES), F32)
    for j in range(D // LANES):
        blend = blend + hidden[:, j * LANES:(j + 1) * LANES].astype(F32) * scorer[j:j + 1]
    blend = jnp.sum(blend, axis=-1, keepdims=True)
    blend = 1.0 / (1.0 + jnp.exp(-blend))

    arrive(got_m)
    smalls[15].wait()
    owners = [mmr[g * max(1, T // GROUPS)].astype(F32) for g in range(GROUPS)]
    for s in range(S):
        for g in range(GROUPS):
            pair = jnp.concatenate([owners[g][s:s + 1, 0:STATE], owners[g][s:s + 1, STATE:M]], axis=0)
            access_new[s, 2, :, g * STATE:(g + 1) * STATE] = pair.astype(BF)

    def relay(j):
        q = lax.rem(mt + j, T)
        here, beside = pieces[j]
        passed = [beside]
        for m in range(1, chips):
            here[m - 1].wait_recv()
            source = lax.rem(me + E - 2 * m, E)
            block = hbuf.at[q, source]
            passed.append(remote(block, block, s_h.at[j, 2 * m + 1], r_h.at[j, 2 * m + 1], {"ep": twin}))
        return passed

    passed = relay(0)
    got_d = None
    tile = tile_of(FFL)
    for c in loads[6:10]:
        c.wait()
    for j in range(T):
        q = lax.rem(mt + j, T)
        arrive(passed)
        here = hbuf[q].reshape(E * S, DS)
        if j == 0:
            dps[:, 0] = dot(here, dg[...]).astype(BF).reshape(T, R, U)
            dps[:, 1] = dot(here, du[...]).astype(BF).reshape(T, R, U)
            dpr[mt] = dps[mt]
            got_d = tp_send(2, lambda to: dps.at[to], dpr.at[mt])
        rows_q = pl.ds(pl.multiple_of(q * DS, DS), DS)
        picked = dot(sel[...], here).astype(BF)

        @pl.loop(0, FFL // tile)
        def _(n, picked=picked, rows_q=rows_q, j=j):
            at = pl.ds(pl.multiple_of(n * tile, tile), tile)
            g = dot(picked, eg[rows_q, at])
            u = dot(picked, eu[rows_q, at])
            if j > 0:
                g = g + gacc[:, at]
                u = u + uacc[:, at]
            if j < T - 1:
                gacc[:, at] = g
                uacc[:, at] = u
            else:
                actb[:, at] = (silu(g) * u).astype(BF)

        if j < T - 1:
            passed = relay(j + 1)

    def dense_act():
        arrive(got_d)
        dsum = dpr[0].astype(F32)
        for j in range(1, T):
            dsum = dsum + dpr[j].astype(F32)
        dab[mt] = (silu(dsum[0]) * dsum[1]).astype(BF)
        return tp_send(3, lambda to: dab.at[mt], dab.at[mt])

    loads[11].wait()
    got_a = None
    got_e = []
    dtile = tile_of(DS)
    for k in range(T - 1, -1, -1):
        to = lax.rem(mt + k, T)
        for n in range(DS // dtile):
            at = pl.ds(pl.multiple_of(to * DS + n * dtile, dtile), dtile)
            share = dot(actb[...], ed[:, at])
            for s in range(E):
                es[k, s, :, n * dtile:(n + 1) * dtile] = share[s * CAP:(s + 1) * CAP].astype(BF)
        for d in range(E - 1, -1, -1):
            owner = lax.rem(me + d, E)
            if k > 0 or d > 0:
                got_e.append(remote(
                    es.at[k, owner], er.at[k, me], s_x.at[k, d], r_x.at[k, d], {"ep": owner, "tp": to}))
            else:
                er[0, me] = es[0, me]
        if k == T - 1:
            got_a = dense_act()
    loads[10].wait()
    arrive(got_a)
    fs[...] = dot(dab[...].reshape(E * S, U), dd[...]).astype(BF).reshape(E, S, DS)
    fr[me] = fs[me]
    got = ep_send(3, lambda to: fs.at[to], fr.at[me])
    arrive(got_e)
    total = er[0].astype(F32)
    for k in range(1, T):
        total = total + er[k].astype(F32)
    outs = total.reshape(N, DS).astype(BF)
    final = rbuf[mt] + dot(mix_hi, outs) + dot(mix_lo, outs)
    arrive(got)
    dense = fr[0].astype(F32)
    for j in range(1, E):
        dense = dense + fr[j].astype(F32)
    out[...] = final + blend * dense
    for c in sends:
        c.wait_send()


def finish(out, rec, inner, access, out_o, rec_o, inner_o, access_o, sem):
    S = rec.shape[0]
    parts = 4 if S % 4 == 0 else 1
    size = S // parts
    copies = [
        pltpu.make_async_copy(rec.at[i * size:(i + 1) * size], rec_o.at[i * size:(i + 1) * size], sem.at[i])
        for i in range(parts)
    ]
    for i, (a, b) in enumerate([(out, out_o), (inner, inner_o), (access, access_o)]):
        copies.append(pltpu.make_async_copy(a, b, sem.at[parts + i]))
    for c in copies:
        c.start()
    for c in copies:
        c.wait()


def local(
    E, T,
    tokens, mix_gain, gate_weight, inner_weight, write_weight, read_weight, step_weight, step_bias,
    decay_log, skip_scale, inner_taps, access_taps, inner_history, access_history, recurrent,
    head_gain, mixer_out, moe_gain, expert_ids, route_scores, expert_gate, expert_up, expert_down,
    blend_vector, dense_gate, dense_up, dense_down,
):
    S, D = tokens.shape
    C = gate_weight.shape[1]
    DC, DS = D // E, D // T
    U = dense_gate.shape[1]
    FFL = expert_gate.shape[2]
    GS = access_taps.shape[2]
    rows = E * S
    R = rows // T
    M = 2 * STATE
    PW = M + LANES + C
    CAP = max(1, 2 * TOP * S // E)
    N = E * CAP
    vmem = pl.BlockSpec(memory_space=pltpu.VMEM)
    hbm = pl.BlockSpec(memory_space=pltpu.HBM)
    V = pltpu.VMEM
    DMA = pltpu.SemaphoreType.DMA
    shapes = (
        jax.ShapeDtypeStruct((S, DS), F32),
        jax.ShapeDtypeStruct((S, C, STATE), F32),
        jax.ShapeDtypeStruct((3, S, C), BF),
        jax.ShapeDtypeStruct((S, 3, 2, GS), BF),
    )
    held = tuple(pltpu.VMEM(x.shape, x.dtype) for x in shapes)
    operands = (
        tokens, mix_gain[None], step_weight.T, step_bias[None], decay_log[None], skip_scale[None],
        inner_taps, access_taps, inner_history.transpose(1, 0, 2), access_history.transpose(0, 2, 1, 3),
        head_gain[None], moe_gain[None], expert_ids.T, route_scores.T, blend_vector.reshape(-1, LANES),
        gate_weight, inner_weight, write_weight, read_weight,
        recurrent.reshape(S, C, STATE), mixer_out,
        expert_gate[0], expert_up[0], expert_down[0], dense_gate, dense_up, dense_down,
    )
    results = pl.pallas_call(
        functools.partial(kernel, E, T, CAP),
        name="decode_step",
        out_shape=held,
        in_specs=[hbm] * 27,
        out_specs=(vmem,) * 4,
        scratch_shapes=[
            V((S, D), BF), V((1, D), F32), V((HEADS, DC), BF), V((1, HEADS), F32), V((1, HEADS), F32),
            V((1, HEADS), F32), V((4, C), BF), V((2, 4, STATE), BF), V((3, S, C), BF), V((S, 3, 2, STATE), BF),
            V((1, C), F32), V((1, D), F32), V((TOP, S), jnp.int32), V((TOP, S), F32), V((D // LANES, LANES), BF),
            V((DC, C), BF), V((DC, C), BF), V((DC, STATE), BF), V((DC, STATE), BF),
            V((S, C, STATE), F32), V((C, D), BF),
            V((D, FFL), BF), V((D, FFL), BF), V((FFL, D), BF),
            V((DS, U), BF), V((DS, U), BF), V((U, DS), BF),
            V((E, S, DC + LANES), BF), V((E, S, DC + LANES), BF), V((E, S, PW), BF), V((E, S, PW), BF),
            V((E, S, C), BF), V((E, S, C), BF), V((S, C, M), BF),
            V((S, D), BF), V((T, S, D), BF), V((S, M), BF), V((T, S, M), BF),
            V((T, S, DS), F32), V((T, E, S, DS), BF),
            V((N, rows), BF), V((N, FFL), F32), V((N, FFL), F32), V((N, FFL), BF),
            V((T, 2, R, U), BF), V((T, 2, R, U), BF), V((T, R, U), BF),
            V((T, E, CAP, DS), BF), V((T, E, CAP, DS), BF),
            V((E, S, DS), BF), V((E, S, DS), BF),
            DMA((16,)), DMA((12,)), DMA((4, E)), DMA((4, E)), DMA((4, T)), DMA((4, T)),
            DMA((T, E)), DMA((T, E)), DMA((T, E)), DMA((T, E)),
        ],
        compiler_params=pltpu.CompilerParams(
            collective_id=0, has_side_effects=True, vmem_limit_bytes=40 * 1024 * 1024
        ),
    )(*[pltpu.with_memory_space_constraint(x, pltpu.HBM) for x in operands])
    out, new_recurrent, inner_new, access_new = pl.pallas_call(
        finish,
        name="store_results",
        out_shape=shapes,
        in_specs=[vmem] * 4,
        out_specs=(hbm,) * 4,
        scratch_shapes=[DMA((8,))],
    )(*[pltpu.with_memory_space_constraint(x, pltpu.VMEM) for x in results])
    return (
        out, new_recurrent.reshape(recurrent.shape), inner_new.transpose(1, 0, 2),
        access_new.transpose(0, 2, 1, 3),
    )


def solution(mesh):
    in_specs = (
        P("ep", None), P(), P("ep", "tp"), P("ep", "tp"), P("ep", None), P("ep", None),
        P("ep", None), P(), P(), P(), P(None, "tp"), P(), P("ep", None, "tp"),
        P("ep", None, None, None), P("ep", "tp", None, None), P("tp"), P("tp", None), P(),
        P("ep", None), P("ep", None), P("ep", None, "tp"), P("ep", None, "tp"),
        P("ep", "tp", None), P(), P("tp", "ep"), P("tp", "ep"), P("ep", "tp"),
    )
    out_specs = (
        P("ep", "tp"), P("ep", "tp", None, None), P("ep", None, "tp"), P("ep", None, None, None),
    )
    body = functools.partial(local, mesh.shape["ep"], mesh.shape["tp"])
    return jax.shard_map(body, mesh=mesh, in_specs=in_specs, out_specs=out_specs, check_vma=False)
```

time: 65.9 us -> 51.2 us (0.78)
  local copies, waits for them, and re-layouts: 7.14 us -> 0 us
  Pallas kernels: 55.4 us -> 50.4 us
  other arithmetic: 2.24 us -> 0 us
    unnamed x6 -> x0, local copies, waits for them, and re-layouts: 5.75 us -> none
    pallas_call x1 -> x2, Pallas kernels: 55.4 us -> 50.4 us  [the longest x1 49 us: local(): pl.pallas_call(functools.partial(kernel, E, T, CAP), name='decode_step',...]
    reshape x2 -> x0, local copies, waits for them, and re-layouts: 0.8 us -> none  [the longest x1 0.78 us: local(): maps = maps_all[::max(1, T // GROUPS)].reshape(-1, S, 2, STATE)]
    reduce_sum x1 -> x0, other arithmetic: 0.78 us -> none  [local(): jnp.sum(hist.astype(F32) * taps[None, :, :3], axis=2).reshape(S, M)]
    concatenate x1 -> x0, other arithmetic: 0.77 us -> none  [local(): new_access = jnp.concatenate([access_history[:, :, 1:], maps], axis=2)]
    convert_element_type x1 -> x0, other arithmetic: 0.69 us -> none  [local(): lax.dynamic_slice_in_dim(access_taps, group * STATE, STATE, 2).astype(F32)]
where the time goes in v1:
time: 51.2 us; the launch traced here: 51.1 us
  Pallas kernels  50.4 us (98%)
  between operations  0.65 us (1%)
    pallas_call x1, Pallas kernels, local(): pl.pallas_call(functools.partial(kernel, E, T, CAP), name='decode_step',...  49 us
    pallas_call x1, Pallas kernels, local(): pl.pallas_call(finish, name='store_results', out_shape=shapes, in_specs=[...  1.42 us

profile of v1, /device:TPU:0, one launch (start us, length us, event | category | flops | bytes accessed | tf_op | source)
XLA Modules:
  0.0 51.1 jit_solution(2347420756913524005)
XLA Ops:
  0.6 49.0 %decode_step.1 = (f32[16,512]{1,0:T(8,128)S(1)}, f32[16,256,128]{2,1,0:T(8,128)S(1)}, bf16[3,16,256]{2,1,0:T(8,128)(2,1)S(1)}, bf16[16,3,2,512]{3,2,1,0:T(2,128)(2,1)S(1)}) custom-call(bf16[16,2048]{1,0:T(8,128)(2,1)} %tokens_h.1, f32[1,2048]{1,0:T(1,128)} %bitcast.25, bf16[16,256]{1,0:T(8,128)(2,1)} %bitcast.26, f32[1,16]{1,0:T(1,128)} %bitcast.32, ...), custom_call_target="tpu_custom_call" | custom-call | tf_op jit(solution)/shard_map/decode_step/pallas_call | solution.py:464
  49.6 1.4 %store_results.1 = (f32[16,512]{1,0:T(8,128)}, f32[16,256,128]{2,1,0:T(8,128)}, bf16[3,16,256]{2,1,0:T(8,128)(2,1)}, bf16[16,3,2,512]{3,2,1,0:T(2,128)(2,1)}) custom-call(f32[16,512]{1,0:T(8,128)S(1)} %get-tuple-element.12.out, f32[16,256,128]{2,1,0:T(8,128)S(1)} %get-tuple-element.13.rec, bf16[3,16,256]{2,1,0:T(8,128)(2,1)S(1)} %get-tuple-element.14.inner, ...), custom_call_target="tpu_custom_call" | custom-call | tf_op jit(solution)/shard_map/store_results/pallas_call | solution.py:493

commit v2 on v1

--- a/solution.py
+++ b/solution.py
@@ -1,4 +1,5 @@
 import functools
+import math
 
 import jax
 import jax.numpy as jnp
@@ -39,8 +40,8 @@
     tokens, mix_gain, step_weight, step_bias, decay_log, skip_scale, inner_taps, access_taps,
     inner_past, access_past, head_gain, moe_gain, ids, scores, blend_vector,
     gw, iw, ww, rw, rec, mw, eg, eu, ed, dg, du, dd,
-    xs, xr, ps, pr, pg, pgr, rcat, ms, mr, mm, mmr, rbuf, hbuf, sel, gacc, uacc, actb, dps, dpr, dab, es, er, fs, fr,
-    small_sem, load_sem, s_ep, r_ep, s_tp, r_tp, s_h, r_h, s_x, r_x,
+    xs, xr, rk, rkr, ps, pr, pg, pgr, rcat, ms, mr, mm, mmr, rbuf, hbuf, sel, cs, cr, gacc, uacc, actb, dps, dpr, dab, es, er, fs, fr,
+    small_sem, load_sem, s_ep, r_ep, s_tp, r_tp, s_h, r_h, s_x, r_x, s_c, r_c, s_d, r_d,
 ):
     me = lax.axis_index("ep")
     mt = lax.axis_index("tp")
@@ -50,7 +51,6 @@
     DS = D // T
     U = dg.shape[1]
     FFL = eg.shape[1]
-    R = E * S // T
     N = E * CAP
     M = 2 * STATE
     group = mt * (HEADS // T) // (HEADS // GROUPS)
@@ -78,14 +78,25 @@
         (dd_w, dd), (ed_w, ed),
     ]
     loads = [pltpu.make_async_copy(a, b, load_sem.at[i]) for i, (a, b) in enumerate(pairs)]
-    for c in smalls[:4]:
+    for c in smalls + loads[:4]:
         c.start()
-    for c in loads[:4]:
-        c.start()
-    for c in smalls[4:]:
-        c.start()
-    for c in loads[4:]:
-        c.start()
+
+    Z = E // 2
+    z, core = me // 2, lax.rem(me, 2)
+    high = 2 * z // Z
+    X = math.isqrt(T) if math.isqrt(T) ** 2 == T else T
+    ty, tx = mt // X, lax.rem(mt, X)
+    shifts = [(dy, dx) for dy in range(T // X) for dx in range(X)]
+    by_reach = sorted(shifts[1:], key=lambda o: -(o[0] > 0) - (o[1] > 0))
+
+    def across(o, sign=1):
+        return lax.rem(ty + sign * o[0] + T // X, T // X) * X + lax.rem(tx + sign * o[1] + X, X)
+
+    def in_order(i):
+        return (1 - high) * (Z - i) + high * i
+
+    def chip_at(dz, dc):
+        return lax.rem(z + dz, Z) * 2 + lax.rem(core + dc, 2)
 
     sends = []
 
@@ -97,17 +108,37 @@
         sends.append(c)
         return c
 
+    def expect(src, dst, send, recv, device):
+        c = pltpu.make_async_remote_copy(
+            src_ref=src, dst_ref=dst, send_sem=send, recv_sem=recv,
+            device_id=device, device_id_type=pl.DeviceIdType.MESH)
+        sends.append(c)
+        return c
+
+    def launch(src, dst, send, recv, device):
+        pltpu.make_async_remote_copy(
+            src_ref=src, dst_ref=dst, send_sem=send, recv_sem=recv,
+            device_id=device, device_id_type=pl.DeviceIdType.MESH).start()
+
+    def ep_expect(phase, src, dst):
+        return [
+            expect(src, dst, s_ep.at[phase, k], r_ep.at[phase, k], {"ep": chip_at(0, 1)}) for k in range(1, E)
+        ]
+
     def ep_send(phase, src_of, dst):
-        got = []
-        for k in range(1, E):
-            to = lax.rem(me + k, E)
-            got.append(remote(src_of(to), dst, s_ep.at[phase, k], r_ep.at[phase, k], {"ep": to}))
-        return got
+        for i in range(1, Z):
+            dz = in_order(i)
+            for dc in range(2):
+                to, k = chip_at(dz, dc), 2 * dz + dc
+                launch(src_of(to), dst, s_ep.at[phase, k], r_ep.at[phase, k], {"ep": to})
+        to = chip_at(0, 1)
+        launch(src_of(to), dst, s_ep.at[phase, 1], r_ep.at[phase, 1], {"ep": to})
+        return ep_expect(phase, src_of(to), dst)
 
     def tp_send(phase, src_of, dst):
         got = []
-        for k in range(1, T):
-            to = lax.rem(mt + k, T)
+        for o in by_reach:
+            to, k = across(o), shifts.index(o)
             got.append(remote(src_of(to), dst, s_tp.at[phase, k], r_tp.at[phase, k], {"tp": to}))
         return got
 
@@ -136,11 +167,15 @@
     before = dot(earlier, named)
     rank = jnp.where(named > 0.0, before, -1.0)
     for j in range(E):
-        xs[j, :, 0:DC] = normed[:, j * DC:(j + 1) * DC]
-        xs[j, :, DC:DC + LANES] = jnp.broadcast_to(rank[:, j:j + 1], (S, LANES)).astype(BF)
+        xs[j] = normed[:, j * DC:(j + 1) * DC]
     xr[me] = xs[me]
+    rk[...] = rank.astype(BF)
+    rkr[me] = rk[...]
     pl.semaphore_wait(barrier, (E - 1) + (T - 1))
-    got = ep_send(0, lambda to: xs.at[to], xr.at[me])
+    ep_send(0, lambda to: xs.at[to], xr.at[me])
+    got_k = ep_send(4, lambda to: rk, rkr.at[me])
+    for c in loads[4:6]:
+        c.start()
 
     for c in smalls[3:15]:
         c.wait()
@@ -150,11 +185,15 @@
     slot = lax.broadcasted_iota(jnp.int32, (S, N), 1)
     slot_rank = lax.rem(slot, CAP).astype(F32)
     mix = jnp.zeros((S, N), F32)
+    hits = jnp.zeros((S, N), F32)
     for e in range(E):
         hit = (slot // CAP == e) & (slot_rank == rank[:, e:e + 1])
         mix = jnp.where(hit, combine[:, e:e + 1], mix)
+        hits = jnp.where(hit, 1.0, hits)
     mix_hi = mix.astype(BF)
     mix_lo = (mix - mix_hi.astype(F32)).astype(BF)
+
+    picker = jnp.transpose(hits).astype(BF)
 
     taps_k = access_taps[...].astype(F32)
     tap_rows = [jnp.concatenate([taps_k[0, k:k + 1], taps_k[1, k:k + 1]], axis=0) for k in range(4)]
@@ -170,26 +209,57 @@
 
     for c in loads[:4]:
         c.wait()
-    arrive(got)
-
-    rows = xr[:, :, 0:DC].reshape(E * S, DC)
-    step_p = lax.dot_general(
-        rows, step_weight[...], (((1,), (1,)), ((), ())), preferred_element_type=F32)
-    step_hi = step_p.astype(BF)
-    step_lo = (step_p - step_hi.astype(F32)).astype(BF)
-    ps[:, :, 0:STATE] = dot(rows, ww[...]).astype(BF).reshape(E, S, STATE)
-    ps[:, :, STATE:M] = dot(rows, rw[...]).astype(BF).reshape(E, S, STATE)
-    ps[:, :, M:M + LANES] = jnp.concatenate(
-        [step_hi, step_lo, jnp.zeros((E * S, LANES - 2 * HEADS), BF)], axis=1).reshape(E, S, LANES)
     G = M + LANES
-    ps[:, :, G:G + C] = dot(rows, iw[...]).astype(BF).reshape(E, S, C)
+
+    def project(dz):
+        chip = lax.rem(z + Z - dz, Z)
+        pair = pl.ds(2 * chip, 2)
+        rows = xr[pair].reshape(2 * S, DC)
+        step_p = lax.dot_general(
+            rows, step_weight[...], (((1,), (1,)), ((), ())), preferred_element_type=F32)
+        step_hi = step_p.astype(BF)
+        step_lo = (step_p - step_hi.astype(F32)).astype(BF)
+        ps[pair, :, 0:STATE] = dot(rows, ww[...]).astype(BF).reshape(2, S, STATE)
+        ps[pair, :, STATE:M] = dot(rows, rw[...]).astype(BF).reshape(2, S, STATE)
+        ps[pair, :, M:G] = jnp.concatenate(
+            [step_hi, step_lo, jnp.zeros((2 * S, LANES - 2 * HEADS), BF)], axis=1).reshape(2, S, LANES)
+        ps[pair, :, G:G + C] = dot(rows, iw[...]).astype(BF).reshape(2, S, C)
+        pg[pair] = dot(rows, gw[...]).astype(BF).reshape(2, S, C)
+
+    def answer(phase, src, dst, back, dc):
+        to, k = chip_at(back, dc), 2 * back + dc
+        launch(src.at[to], dst.at[me], s_ep.at[phase, k], r_ep.at[phase, k], {"ep": to})
+
+    def normed_from(dz, dc):
+        k = 2 * dz + dc
+        return pltpu.make_async_remote_copy(
+            src_ref=xs.at[0], dst_ref=xr.at[0], send_sem=s_ep.at[0, k], recv_sem=r_ep.at[0, k],
+            device_id={"ep": chip_at(0, 1)}, device_id_type=pl.DeviceIdType.MESH)
+
+    normed_from(0, 1).wait_recv()
+    project(0)
+    answer(1, ps, pr, 0, 1)
+    answer(2, pg, pgr, 0, 1)
     pr[me] = ps[me]
-    got = ep_send(1, lambda to: ps.at[to], pr.at[me])
-    pg[...] = dot(rows, gw[...]).astype(BF).reshape(E, S, C)
     pgr[me] = pg[me]
-    got_g = ep_send(2, lambda to: pg.at[to], pgr.at[me])
-
-    rank_of = xr[:, :, DC:DC + LANES].reshape(E * S, LANES)[:, 0:N].astype(F32)
+    for i in range(1, Z):
+        dz = in_order(i)
+        for dc in range(2):
+            normed_from(dz, dc).wait_recv()
+        project(dz)
+        for dc in range(2):
+            answer(1, ps, pr, Z - dz, dc)
+        for dc in range(2):
+            answer(2, pg, pgr, Z - dz, dc)
+    got = ep_expect(1, ps.at[0], pr.at[0])
+    got_g = ep_expect(2, pg.at[0], pgr.at[0])
+    for c in loads[6:]:
+        c.start()
+    arrive(got_k)
+
+    every = rkr[...].reshape(E * S, LANES).astype(F32)
+    expert_lane = lax.broadcasted_iota(jnp.int32, (E * S, LANES), 1)
+    rank_of = jnp.sum(jnp.where(expert_lane == me, every, 0.0), axis=-1, keepdims=True)
     wide = lax.broadcasted_iota(jnp.int32, (E * S, N), 1)
     seq = lax.broadcasted_iota(jnp.int32, (E * S, N), 0)
     chosen = (wide // CAP == seq // S) & (lax.rem(wide, CAP).astype(F32) == rank_of)
@@ -287,17 +357,28 @@
         rbuf[q] = resid[:, q * DS:(q + 1) * DS]
         hbuf[q, me] = hidden[:, q * DS:(q + 1) * DS]
 
-    twin = me + 1 - 2 * lax.rem(me, 2)
-    chips = E // 2
-    pieces = []
-    for j in range(T):
-        q = lax.rem(mt + j, T)
-        here = []
-        for m in range(1, chips):
-            to = lax.rem(me + 2 * m, E)
-            here.append(remote(hbuf.at[q, me], hbuf.at[q, me], s_h.at[j, 2 * m], r_h.at[j, 2 * m], {"ep": to}))
-        beside = remote(hbuf.at[q, me], hbuf.at[q, me], s_h.at[j, 1], r_h.at[j, 1], {"ep": twin})
-        pieces.append((here, beside))
+    twin = chip_at(0, 1)
+    for i in range(1, Z):
+        dz = in_order(i)
+        launch(hbuf.at[mt, me], hbuf.at[mt, me], s_h.at[2 * dz], r_h.at[2 * dz], {"ep": chip_at(dz, 0)})
+    beside = remote(hbuf.at[mt, me], hbuf.at[mt, me], s_h.at[1], r_h.at[1], {"ep": twin})
+    for q in range(T):
+        chosen_q = dot(picker, hidden[:, q * DS:(q + 1) * DS])
+        for e in range(E):
+            cs[q, e] = chosen_q[e * CAP:(e + 1) * CAP].astype(BF)
+    got_c = []
+    for o in by_reach:
+        q, n = across(o), shifts.index(o)
+        cr[q, me] = cs[q, me]
+        for i in range(1, Z + 1):
+            dz = in_order(i) if i < Z else 0
+            for dc in range(2):
+                if i < Z or dc > 0:
+                    to, k = chip_at(dz, dc), 2 * dz + dc
+                    launch(cs.at[q, to], cr.at[q, me], s_c.at[n, k], r_c.at[n, k], {"ep": to})
+        got_c.append([
+            expect(cs.at[q, 0], cr.at[q, 0], s_c.at[n, k], r_c.at[n, k], {"ep": twin}) for k in range(1, E)
+        ])
 
     scorer = blend_vector[...].astype(F32)
     blend = jnp.zeros((S, LANES), F32)
@@ -314,82 +395,117 @@
             pair = jnp.concatenate([owners[g][s:s + 1, 0:STATE], owners[g][s:s + 1, STATE:M]], axis=0)
             access_new[s, 2, :, g * STATE:(g + 1) * STATE] = pair.astype(BF)
 
-    def relay(j):
-        q = lax.rem(mt + j, T)
-        here, beside = pieces[j]
-        passed = [beside]
-        for m in range(1, chips):
-            here[m - 1].wait_recv()
-            source = lax.rem(me + E - 2 * m, E)
-            block = hbuf.at[q, source]
-            passed.append(remote(block, block, s_h.at[j, 2 * m + 1], r_h.at[j, 2 * m + 1], {"ep": twin}))
-        return passed
-
-    passed = relay(0)
-    got_d = None
-    tile = tile_of(FFL)
-    for c in loads[6:10]:
-        c.wait()
-    for j in range(T):
-        q = lax.rem(mt + j, T)
-        arrive(passed)
-        here = hbuf[q].reshape(E * S, DS)
-        if j == 0:
-            dps[:, 0] = dot(here, dg[...]).astype(BF).reshape(T, R, U)
-            dps[:, 1] = dot(here, du[...]).astype(BF).reshape(T, R, U)
-            dpr[mt] = dps[mt]
-            got_d = tp_send(2, lambda to: dps.at[to], dpr.at[mt])
+    def piece(dz, dc):
+        k = 2 * dz + dc
+        block = hbuf.at[mt, chip_at(Z - dz, dc)]
+        return pltpu.make_async_remote_copy(
+            src_ref=block, dst_ref=block, send_sem=s_h.at[k], recv_sem=r_h.at[k],
+            device_id={"ep": twin}, device_id_type=pl.DeviceIdType.MESH)
+
+    def relay(i):
+        dz = in_order(i)
+        piece(dz, 0).wait_recv()
+        block = hbuf.at[mt, chip_at(Z - dz, 0)]
+        launch(block, block, s_h.at[2 * dz + 1], r_h.at[2 * dz + 1], {"ep": twin})
+
+    def passed(i):
+        piece(in_order(i), 1).wait_recv()
+
+    Q = 2 * S // T
+
+    def dense_part(dz):
+        chip = lax.rem(z + Z - dz, Z)
+        here = hbuf[mt, pl.ds(2 * chip, 2)].reshape(2 * S, DS)
+        for w, weight in enumerate((dg, du)):
+            part = dot(here, weight[...])
+            for m in range(T):
+                dps[chip, m, w] = part[m * Q:(m + 1) * Q].astype(BF)
+        for o in by_reach:
+            to, k = across(o), shifts.index(o)
+            launch(dps.at[chip, to], dpr.at[mt, chip], s_d.at[k, dz], r_d.at[k, dz], {"tp": to})
+        dpr[mt, chip] = dps[chip, mt]
+
+    def expert_part(picked, q, first, last):
         rows_q = pl.ds(pl.multiple_of(q * DS, DS), DS)
-        picked = dot(sel[...], here).astype(BF)
-
-        @pl.loop(0, FFL // tile)
-        def _(n, picked=picked, rows_q=rows_q, j=j):
-            at = pl.ds(pl.multiple_of(n * tile, tile), tile)
+        for n in range(FFL // tile):
+            at = slice(n * tile, (n + 1) * tile)
             g = dot(picked, eg[rows_q, at])
             u = dot(picked, eu[rows_q, at])
-            if j > 0:
+            if not first:
                 g = g + gacc[:, at]
                 u = u + uacc[:, at]
-            if j < T - 1:
+            if last:
+                actb[:, at] = (silu(g) * u).astype(BF)
+            else:
                 gacc[:, at] = g
                 uacc[:, at] = u
-            else:
-                actb[:, at] = (silu(g) * u).astype(BF)
-
-        if j < T - 1:
-            passed = relay(j + 1)
+
+    tile = tile_of(FFL)
+    for c in loads[6:8]:
+        c.wait()
+    beside.wait_recv()
+    dense_part(0)
+    for i in range(1, Z):
+        relay(i)
+        if i > 1:
+            passed(i - 1)
+            dense_part(in_order(i - 1))
+    passed(Z - 1)
+    dense_part(in_order(Z - 1))
+    got_d = [
+        expect(dps.at[0, 0], dpr.at[0, 0], s_d.at[k, d], r_d.at[k, d], {"tp": lax.rem(mt + k, T)})
+        for k in range(1, T) for d in range(Z)
+    ]
+    for c in loads[8:10]:
+        c.wait()
+    own = dot(sel[...], hbuf[mt].reshape(E * S, DS)).astype(BF)
+    expert_part(own, mt, True, T == 1)
+    for n, o in enumerate(by_reach):
+        q = across(o)
+        arrive(got_c[n])
+        picked = cr[q].astype(F32).reshape(N, DS).astype(BF)
+        expert_part(picked, q, False, n == len(by_reach) - 1)
 
     def dense_act():
         arrive(got_d)
-        dsum = dpr[0].astype(F32)
-        for j in range(1, T):
-            dsum = dsum + dpr[j].astype(F32)
-        dab[mt] = (silu(dsum[0]) * dsum[1]).astype(BF)
-        return tp_send(3, lambda to: dab.at[mt], dab.at[mt])
+        for chip in range(Z):
+            dsum = dpr[0, chip].astype(F32)
+            for j in range(1, T):
+                dsum = dsum + dpr[j, chip].astype(F32)
+            dab[mt, chip] = (silu(dsum[0]) * dsum[1]).astype(BF)
+        return tp_send(2, lambda to: dab.at[mt], dab.at[mt])
 
     loads[11].wait()
+    got_e = []
     got_a = None
-    got_e = []
     dtile = tile_of(DS)
-    for k in range(T - 1, -1, -1):
-        to = lax.rem(mt + k, T)
+    for o in by_reach + shifts[:1]:
+        to, k = across(o), shifts.index(o)
         for n in range(DS // dtile):
             at = pl.ds(pl.multiple_of(to * DS + n * dtile, dtile), dtile)
             share = dot(actb[...], ed[:, at])
             for s in range(E):
                 es[k, s, :, n * dtile:(n + 1) * dtile] = share[s * CAP:(s + 1) * CAP].astype(BF)
-        for d in range(E - 1, -1, -1):
-            owner = lax.rem(me + d, E)
+        for i in range(1, Z + 1):
+            dz = in_order(i) if i < Z else 0
+            for dc in range(2):
+                owner, d = chip_at(dz, dc), 2 * dz + dc
+                if i == Z and dc == 0 and k == 0:
+                    er[0, me] = es[0, me]
+                else:
+                    launch(es.at[k, owner], er.at[k, me], s_x.at[k, d], r_x.at[k, d], {"ep": owner, "tp": to})
+        for d in range(E):
             if k > 0 or d > 0:
-                got_e.append(remote(
-                    es.at[k, owner], er.at[k, me], s_x.at[k, d], r_x.at[k, d], {"ep": owner, "tp": to}))
-            else:
-                er[0, me] = es[0, me]
-        if k == T - 1:
+                got_e.append(expect(es.at[k, 0], er.at[k, 0], s_x.at[k, d], r_x.at[k, d], {"ep": twin, "tp": to}))
+        if o == by_reach[min(1, T - 2)]:
             got_a = dense_act()
     loads[10].wait()
     arrive(got_a)
-    fs[...] = dot(dab[...].reshape(E * S, U), dd[...]).astype(BF).reshape(E, S, DS)
+    shares = dot(dab[...].astype(F32).reshape(E * S, U).astype(BF), dd[...])
+    for m in range(T):
+        for chip in range(Z):
+            base = (m * Z + chip) * Q
+            fs[2 * chip + m * Q // S, m * Q % S:m * Q % S + Q] = shares[base:base + Q].astype(BF)
     fr[me] = fs[me]
     got = ep_send(3, lambda to: fs.at[to], fr.at[me])
     arrive(got_e)
@@ -403,6 +519,8 @@
     for j in range(1, E):
         dense = dense + fr[j].astype(F32)
     out[...] = final + blend * dense
+    for k in range(2, E):
+        piece(k // 2, k % 2).wait_send()
     for c in sends:
         c.wait_send()
 
@@ -437,7 +555,8 @@
     FFL = expert_gate.shape[2]
     GS = access_taps.shape[2]
     rows = E * S
-    R = rows // T
+    Z = E // 2
+    Q = 2 * S // T
     M = 2 * STATE
     PW = M + LANES + C
     CAP = max(1, 2 * TOP * S // E)
@@ -475,16 +594,16 @@
             V((S, C, STATE), F32), V((C, D), BF),
             V((D, FFL), BF), V((D, FFL), BF), V((FFL, D), BF),
             V((DS, U), BF), V((DS, U), BF), V((U, DS), BF),
-            V((E, S, DC + LANES), BF), V((E, S, DC + LANES), BF), V((E, S, PW), BF), V((E, S, PW), BF),
+            V((E, S, DC), BF), V((E, S, DC), BF), V((S, LANES), BF), V((E, S, LANES), BF), V((E, S, PW), BF), V((E, S, PW), BF),
             V((E, S, C), BF), V((E, S, C), BF), V((S, C, M), BF),
             V((S, D), BF), V((T, S, D), BF), V((S, M), BF), V((T, S, M), BF),
             V((T, S, DS), F32), V((T, E, S, DS), BF),
-            V((N, rows), BF), V((N, FFL), F32), V((N, FFL), F32), V((N, FFL), BF),
-            V((T, 2, R, U), BF), V((T, 2, R, U), BF), V((T, R, U), BF),
+            V((N, rows), BF), V((T, E, CAP, DS), BF), V((T, E, CAP, DS), BF), V((N, FFL), F32), V((N, FFL), F32), V((N, FFL), BF),
+            V((Z, T, 2, Q, U), BF), V((T, Z, 2, Q, U), BF), V((T, Z, Q, U), BF),
             V((T, E, CAP, DS), BF), V((T, E, CAP, DS), BF),
             V((E, S, DS), BF), V((E, S, DS), BF),
-            DMA((16,)), DMA((12,)), DMA((4, E)), DMA((4, E)), DMA((4, T)), DMA((4, T)),
-            DMA((T, E)), DMA((T, E)), DMA((T, E)), DMA((T, E)),
+            DMA((16,)), DMA((12,)), DMA((5, E)), DMA((5, E)), DMA((4, T)), DMA((4, T)),
+            DMA((E,)), DMA((E,)), DMA((T, E)), DMA((T, E)), DMA((T, E)), DMA((T, E)), DMA((T, Z)), DMA((T, Z)),
         ],
         compiler_params=pltpu.CompilerParams(
             collective_id=0, has_side_effects=True, vmem_limit_bytes=40 * 1024 * 1024

time: 51.2 us -> 47.4 us (0.926)
  Pallas kernels: 50.4 us -> 46.6 us
    pallas_call x1, Pallas kernels: 49 us -> 45.2 us  [local(): pl.pallas_call(functools.partial(kernel, E, T, CAP), name='decode_step',...]
where the time goes in v2:
time: 47.4 us; the launch traced here: 47.2 us
  Pallas kernels  46.6 us (98%)
  between operations  0.65 us (1%)
    pallas_call x1, Pallas kernels, local(): pl.pallas_call(functools.partial(kernel, E, T, CAP), name='decode_step',...  45.2 us
    pallas_call x1, Pallas kernels, local(): pl.pallas_call(finish, name='store_results', out_shape=shapes, in_specs=[...  1.42 us

profile of v2, /device:TPU:0, one launch (start us, length us, event | category | flops | bytes accessed | tf_op | source)
XLA Modules:
  0.0 47.2 jit_solution(11258363296056192948)
XLA Ops:
  0.6 45.2 %decode_step.1 = (f32[16,512]{1,0:T(8,128)S(1)}, f32[16,256,128]{2,1,0:T(8,128)S(1)}, bf16[3,16,256]{2,1,0:T(8,128)(2,1)S(1)}, bf16[16,3,2,512]{3,2,1,0:T(2,128)(2,1)S(1)}) custom-call(bf16[16,2048]{1,0:T(8,128)(2,1)} %tokens_h.1, f32[1,2048]{1,0:T(1,128)} %bitcast.25, bf16[16,256]{1,0:T(8,128)(2,1)} %bitcast.26, f32[1,16]{1,0:T(1,128)} %bitcast.32, ...), custom_call_target="tpu_custom_call" | custom-call | tf_op jit(solution)/shard_map/decode_step/pallas_call | solution.py:583
  45.8 1.4 %store_results.1 = (f32[16,512]{1,0:T(8,128)}, f32[16,256,128]{2,1,0:T(8,128)}, bf16[3,16,256]{2,1,0:T(8,128)(2,1)}, bf16[16,3,2,512]{3,2,1,0:T(2,128)(2,1)}) custom-call(f32[16,512]{1,0:T(8,128)S(1)} %get-tuple-element.12.out, f32[16,256,128]{2,1,0:T(8,128)S(1)} %get-tuple-element.13.rec, bf16[3,16,256]{2,1,0:T(8,128)(2,1)S(1)} %get-tuple-element.14.inner, ...), custom_call_target="tpu_custom_call" | custom-call | tf_op jit(solution)/shard_map/store_results/pallas_call | solution.py:612

commit v3 on v2

--- a/solution.py
+++ b/solution.py
@@ -36,12 +36,13 @@
     tokens_h, mix_gain_h, step_weight_h, step_bias_h, decay_log_h, skip_scale_h, inner_taps_h, access_taps_h,
     inner_past_h, access_past_h, head_gain_h, moe_gain_h, ids_h, scores_h, blend_vector_h,
     gate_w, inner_w, write_w, read_w, recurrent, mixer_w, eg_w, eu_w, ed_w, dg_w, du_w, dd_w,
+    out_k, nrec_k, inner_k, access_k,
     out, nrec, inner_new, access_new,
     tokens, mix_gain, step_weight, step_bias, decay_log, skip_scale, inner_taps, access_taps,
     inner_past, access_past, head_gain, moe_gain, ids, scores, blend_vector,
     gw, iw, ww, rw, rec, mw, eg, eu, ed, dg, du, dd,
     xs, xr, rk, rkr, ps, pr, pg, pgr, rcat, ms, mr, mm, mmr, rbuf, hbuf, sel, cs, cr, gacc, uacc, actb, dps, dpr, dab, es, er, fs, fr,
-    small_sem, load_sem, s_ep, r_ep, s_tp, r_tp, s_h, r_h, s_x, r_x, s_c, r_c, s_d, r_d,
+    keep_sem, small_sem, load_sem, sent, r_one, r_n, r_h, r_c, r_d, r_a, r_e,
 ):
     me = lax.axis_index("ep")
     mt = lax.axis_index("tp")
@@ -98,53 +99,38 @@
     def chip_at(dz, dc):
         return lax.rem(z + dz, Z) * 2 + lax.rem(core + dc, 2)
 
-    sends = []
-
-    def remote(src, dst, send, recv, device):
-        c = pltpu.make_async_remote_copy(
-            src_ref=src, dst_ref=dst, send_sem=send, recv_sem=recv,
+    keeps = [
+        pltpu.make_async_copy(a, b, keep_sem.at[i])
+        for i, (a, b) in enumerate([(out, out_k), (nrec, nrec_k), (inner_new, inner_k), (access_new, access_k)])
+    ]
+    NORM, RANK, MAPS, GATE, MIXED, GROUP, HID, PICK, PART, ACT, FAR, NEAR, DENSE = range(13)
+
+    def copy(src, dst, kind, recv, device):
+        return pltpu.make_async_remote_copy(
+            src_ref=src, dst_ref=dst, send_sem=sent.at[kind], recv_sem=recv,
             device_id=device, device_id_type=pl.DeviceIdType.MESH)
-        c.start()
-        sends.append(c)
-        return c
-
-    def expect(src, dst, send, recv, device):
-        c = pltpu.make_async_remote_copy(
-            src_ref=src, dst_ref=dst, send_sem=send, recv_sem=recv,
-            device_id=device, device_id_type=pl.DeviceIdType.MESH)
-        sends.append(c)
-        return c
-
-    def launch(src, dst, send, recv, device):
-        pltpu.make_async_remote_copy(
-            src_ref=src, dst_ref=dst, send_sem=send, recv_sem=recv,
-            device_id=device, device_id_type=pl.DeviceIdType.MESH).start()
-
-    def ep_expect(phase, src, dst):
-        return [
-            expect(src, dst, s_ep.at[phase, k], r_ep.at[phase, k], {"ep": chip_at(0, 1)}) for k in range(1, E)
-        ]
-
-    def ep_send(phase, src_of, dst):
+
+    def launch(*args):
+        copy(*args).start()
+
+    def arrive(ref, recv):
+        copy(ref, ref, NORM, recv, {"ep": chip_at(0, 1)}).wait_recv()
+
+    def leave(ref, kind):
+        copy(ref, ref, kind, r_one.at[0], {"ep": chip_at(0, 1)}).wait_send()
+
+    def ep_send(kind, src_of, dst, recv):
         for i in range(1, Z):
             dz = in_order(i)
             for dc in range(2):
-                to, k = chip_at(dz, dc), 2 * dz + dc
-                launch(src_of(to), dst, s_ep.at[phase, k], r_ep.at[phase, k], {"ep": to})
+                to = chip_at(dz, dc)
+                launch(src_of(to), dst, kind, recv(dz), {"ep": to})
         to = chip_at(0, 1)
-        launch(src_of(to), dst, s_ep.at[phase, 1], r_ep.at[phase, 1], {"ep": to})
-        return ep_expect(phase, src_of(to), dst)
-
-    def tp_send(phase, src_of, dst):
-        got = []
+        launch(src_of(to), dst, kind, recv(0), {"ep": to})
+
+    def tp_send(kind, src, dst, recv):
         for o in by_reach:
-            to, k = across(o), shifts.index(o)
-            got.append(remote(src_of(to), dst, s_tp.at[phase, k], r_tp.at[phase, k], {"tp": to}))
-        return got
-
-    def arrive(copies):
-        for c in copies:
-            c.wait_recv()
+            launch(src, dst, kind, recv, {"tp": across(o)})
 
     lane = lax.broadcasted_iota(jnp.int32, (S, LANES), 1)
     lane_f = lane.astype(F32)
@@ -172,8 +158,8 @@
     rk[...] = rank.astype(BF)
     rkr[me] = rk[...]
     pl.semaphore_wait(barrier, (E - 1) + (T - 1))
-    ep_send(0, lambda to: xs.at[to], xr.at[me])
-    got_k = ep_send(4, lambda to: rk, rkr.at[me])
+    ep_send(NORM, lambda to: xs.at[to], xr.at[me], lambda dz: r_n.at[dz])
+    ep_send(RANK, lambda to: rk, rkr.at[me], lambda dz: r_one.at[0])
     for c in loads[4:6]:
         c.start()
 
@@ -226,36 +212,27 @@
         ps[pair, :, G:G + C] = dot(rows, iw[...]).astype(BF).reshape(2, S, C)
         pg[pair] = dot(rows, gw[...]).astype(BF).reshape(2, S, C)
 
-    def answer(phase, src, dst, back, dc):
-        to, k = chip_at(back, dc), 2 * back + dc
-        launch(src.at[to], dst.at[me], s_ep.at[phase, k], r_ep.at[phase, k], {"ep": to})
-
-    def normed_from(dz, dc):
-        k = 2 * dz + dc
-        return pltpu.make_async_remote_copy(
-            src_ref=xs.at[0], dst_ref=xr.at[0], send_sem=s_ep.at[0, k], recv_sem=r_ep.at[0, k],
-            device_id={"ep": chip_at(0, 1)}, device_id_type=pl.DeviceIdType.MESH)
-
-    normed_from(0, 1).wait_recv()
+    def answer(kind, src, dst, recv, back, dc):
+        to = chip_at(back, dc)
+        launch(src.at[to], dst.at[me], kind, recv, {"ep": to})
+
+    arrive(xr.at[0], r_n.at[0])
     project(0)
-    answer(1, ps, pr, 0, 1)
-    answer(2, pg, pgr, 0, 1)
+    answer(MAPS, ps, pr, r_one.at[1], 0, 1)
+    answer(GATE, pg, pgr, r_one.at[2], 0, 1)
     pr[me] = ps[me]
     pgr[me] = pg[me]
     for i in range(1, Z):
         dz = in_order(i)
-        for dc in range(2):
-            normed_from(dz, dc).wait_recv()
+        arrive(xr.at[0:2], r_n.at[dz])
         project(dz)
         for dc in range(2):
-            answer(1, ps, pr, Z - dz, dc)
+            answer(MAPS, ps, pr, r_one.at[1], Z - dz, dc)
         for dc in range(2):
-            answer(2, pg, pgr, Z - dz, dc)
-    got = ep_expect(1, ps.at[0], pr.at[0])
-    got_g = ep_expect(2, pg.at[0], pgr.at[0])
+            answer(GATE, pg, pgr, r_one.at[2], Z - dz, dc)
     for c in loads[6:]:
         c.start()
-    arrive(got_k)
+    arrive(rkr.at[0:E - 1], r_one.at[0])
 
     every = rkr[...].reshape(E * S, LANES).astype(F32)
     expert_lane = lax.broadcasted_iota(jnp.int32, (E * S, LANES), 1)
@@ -290,7 +267,7 @@
         rcat[t, :, 0:STATE] = high
         rcat[t, :, STATE:M] = (value - high.astype(F32)).astype(BF)
 
-    arrive(got)
+    arrive(pr.at[0:E - 1], r_one.at[1])
     proj = pr[0].astype(F32)
     for j in range(1, E):
         proj = proj + pr[j].astype(F32)
@@ -321,7 +298,7 @@
     read_rows = jnp.transpose(read_t)
     recalled = read_rows[0:S] + read_rows[S:2 * S]
     readout = decay * recalled + push * both + skip * inner
-    arrive(got_g)
+    arrive(pgr.at[0:E - 1], r_one.at[2])
     gate_sum = pgr[0].astype(F32)
     for j in range(1, E):
         gate_sum = gate_sum + pgr[j].astype(F32)
@@ -337,16 +314,18 @@
     for j in range(T):
         ms[:, j * DS:(j + 1) * DS] = dot(head_out, mw[:, j * DS:(j + 1) * DS]).astype(BF)
     mr[mt] = ms[...]
-    got = tp_send(0, lambda to: ms, mr.at[mt])
+    tp_send(MIXED, ms, mr.at[mt], r_one.at[3])
     mmr[mt] = mm[...]
-    got_m = tp_send(1, lambda to: mm, mmr.at[mt])
+    tp_send(GROUP, mm, mmr.at[mt], r_one.at[4])
 
     decay_t = jnp.transpose(decay)
     push_t = jnp.transpose(push)
     for t in range(S):
         nrec[t] = decay_t[:, t:t + 1] * rec[t] + push_t[:, t:t + 1] * write_c[t:t + 1]
-
-    arrive(got)
+    keeps[1].start()
+    keeps[2].start()
+
+    arrive(mr.at[0:T - 1], r_one.at[3])
     mixed = mr[0].astype(F32)
     for j in range(1, T):
         mixed = mixed + mr[j].astype(F32)
@@ -360,13 +339,12 @@
     twin = chip_at(0, 1)
     for i in range(1, Z):
         dz = in_order(i)
-        launch(hbuf.at[mt, me], hbuf.at[mt, me], s_h.at[2 * dz], r_h.at[2 * dz], {"ep": chip_at(dz, 0)})
-    beside = remote(hbuf.at[mt, me], hbuf.at[mt, me], s_h.at[1], r_h.at[1], {"ep": twin})
+        launch(hbuf.at[mt, me], hbuf.at[mt, me], HID, r_h.at[2 * dz], {"ep": chip_at(dz, 0)})
+    launch(hbuf.at[mt, me], hbuf.at[mt, me], HID, r_h.at[1], {"ep": twin})
     for q in range(T):
         chosen_q = dot(picker, hidden[:, q * DS:(q + 1) * DS])
         for e in range(E):
             cs[q, e] = chosen_q[e * CAP:(e + 1) * CAP].astype(BF)
-    got_c = []
     for o in by_reach:
         q, n = across(o), shifts.index(o)
         cr[q, me] = cs[q, me]
@@ -374,11 +352,8 @@
             dz = in_order(i) if i < Z else 0
             for dc in range(2):
                 if i < Z or dc > 0:
-                    to, k = chip_at(dz, dc), 2 * dz + dc
-                    launch(cs.at[q, to], cr.at[q, me], s_c.at[n, k], r_c.at[n, k], {"ep": to})
-        got_c.append([
-            expect(cs.at[q, 0], cr.at[q, 0], s_c.at[n, k], r_c.at[n, k], {"ep": twin}) for k in range(1, E)
-        ])
+                    to = chip_at(dz, dc)
+                    launch(cs.at[q, to], cr.at[q, me], PICK, r_c.at[n], {"ep": to})
 
     scorer = blend_vector[...].astype(F32)
     blend = jnp.zeros((S, LANES), F32)
@@ -387,29 +362,24 @@
     blend = jnp.sum(blend, axis=-1, keepdims=True)
     blend = 1.0 / (1.0 + jnp.exp(-blend))
 
-    arrive(got_m)
+    arrive(mmr.at[0:T - 1], r_one.at[4])
     smalls[15].wait()
     owners = [mmr[g * max(1, T // GROUPS)].astype(F32) for g in range(GROUPS)]
     for s in range(S):
         for g in range(GROUPS):
             pair = jnp.concatenate([owners[g][s:s + 1, 0:STATE], owners[g][s:s + 1, STATE:M]], axis=0)
             access_new[s, 2, :, g * STATE:(g + 1) * STATE] = pair.astype(BF)
-
-    def piece(dz, dc):
-        k = 2 * dz + dc
-        block = hbuf.at[mt, chip_at(Z - dz, dc)]
-        return pltpu.make_async_remote_copy(
-            src_ref=block, dst_ref=block, send_sem=s_h.at[k], recv_sem=r_h.at[k],
-            device_id={"ep": twin}, device_id_type=pl.DeviceIdType.MESH)
+    keeps[3].start()
 
     def relay(i):
         dz = in_order(i)
-        piece(dz, 0).wait_recv()
         block = hbuf.at[mt, chip_at(Z - dz, 0)]
-        launch(block, block, s_h.at[2 * dz + 1], r_h.at[2 * dz + 1], {"ep": twin})
+        arrive(block, r_h.at[2 * dz])
+        launch(block, block, HID, r_h.at[2 * dz + 1], {"ep": twin})
 
     def passed(i):
-        piece(in_order(i), 1).wait_recv()
+        dz = in_order(i)
+        arrive(hbuf.at[mt, chip_at(Z - dz, 1)], r_h.at[2 * dz + 1])
 
     Q = 2 * S // T
 
@@ -421,9 +391,26 @@
             for m in range(T):
                 dps[chip, m, w] = part[m * Q:(m + 1) * Q].astype(BF)
         for o in by_reach:
-            to, k = across(o), shifts.index(o)
-            launch(dps.at[chip, to], dpr.at[mt, chip], s_d.at[k, dz], r_d.at[k, dz], {"tp": to})
+            to = across(o)
+            launch(dps.at[chip, to], dpr.at[mt, chip], PART, r_d.at[dz], {"tp": to})
         dpr[mt, chip] = dps[chip, mt]
+
+    def dense_act(dz):
+        chip = lax.rem(z + Z - dz, Z)
+        arrive(dpr.at[0:T - 1, 0], r_d.at[dz])
+        dsum = dpr[0, chip].astype(F32)
+        for j in range(1, T):
+            dsum = dsum + dpr[j, chip].astype(F32)
+        dab[mt, chip] = (silu(dsum[0]) * dsum[1]).astype(BF)
+        for o in by_reach:
+            launch(dab.at[mt, chip], dab.at[mt, chip], ACT, r_a.at[dz], {"tp": across(o)})
+
+    def dense_down(dz):
+        chip = lax.rem(z + Z - dz, Z)
+        pair = pl.ds(2 * chip, 2)
+        arrive(dab.at[0:T - 1, 0], r_a.at[dz])
+        acts = dab[:, chip].astype(F32).reshape(2 * S, U).astype(BF)
+        fs[pair] = dot(acts, dd[...]).astype(BF).reshape(2, S, DS)
 
     def expert_part(picked, q, first, last):
         rows_q = pl.ds(pl.multiple_of(q * DS, DS), DS)
@@ -443,7 +430,7 @@
     tile = tile_of(FFL)
     for c in loads[6:8]:
         c.wait()
-    beside.wait_recv()
+    arrive(hbuf.at[mt, twin], r_h.at[1])
     dense_part(0)
     for i in range(1, Z):
         relay(i)
@@ -452,32 +439,20 @@
             dense_part(in_order(i - 1))
     passed(Z - 1)
     dense_part(in_order(Z - 1))
-    got_d = [
-        expect(dps.at[0, 0], dpr.at[0, 0], s_d.at[k, d], r_d.at[k, d], {"tp": lax.rem(mt + k, T)})
-        for k in range(1, T) for d in range(Z)
-    ]
     for c in loads[8:10]:
         c.wait()
     own = dot(sel[...], hbuf[mt].reshape(E * S, DS)).astype(BF)
+    dense_act(0)
     expert_part(own, mt, True, T == 1)
     for n, o in enumerate(by_reach):
         q = across(o)
-        arrive(got_c[n])
+        arrive(cr.at[q, 0:E - 1], r_c.at[shifts.index(o)])
         picked = cr[q].astype(F32).reshape(N, DS).astype(BF)
         expert_part(picked, q, False, n == len(by_reach) - 1)
-
-    def dense_act():
-        arrive(got_d)
-        for chip in range(Z):
-            dsum = dpr[0, chip].astype(F32)
-            for j in range(1, T):
-                dsum = dsum + dpr[j, chip].astype(F32)
-            dab[mt, chip] = (silu(dsum[0]) * dsum[1]).astype(BF)
-        return tp_send(2, lambda to: dab.at[mt], dab.at[mt])
+        if n == 1:
+            dense_act(in_order(1))
 
     loads[11].wait()
-    got_e = []
-    got_a = None
     dtile = tile_of(DS)
     for o in by_reach + shifts[:1]:
         to, k = across(o), shifts.index(o)
@@ -489,40 +464,54 @@
         for i in range(1, Z + 1):
             dz = in_order(i) if i < Z else 0
             for dc in range(2):
-                owner, d = chip_at(dz, dc), 2 * dz + dc
+                owner = chip_at(dz, dc)
                 if i == Z and dc == 0 and k == 0:
                     er[0, me] = es[0, me]
                 else:
-                    launch(es.at[k, owner], er.at[k, me], s_x.at[k, d], r_x.at[k, d], {"ep": owner, "tp": to})
-        for d in range(E):
-            if k > 0 or d > 0:
-                got_e.append(expect(es.at[k, 0], er.at[k, 0], s_x.at[k, d], r_x.at[k, d], {"ep": twin, "tp": to}))
-        if o == by_reach[min(1, T - 2)]:
-            got_a = dense_act()
+                    launch(
+                        es.at[k, owner], er.at[k, me], FAR if k > 0 else NEAR, r_e.at[min(k, 1)],
+                        {"ep": owner, "tp": to})
+        if o == by_reach[0]:
+            dense_act(in_order(2))
     loads[10].wait()
-    arrive(got_a)
-    shares = dot(dab[...].astype(F32).reshape(E * S, U).astype(BF), dd[...])
-    for m in range(T):
-        for chip in range(Z):
-            base = (m * Z + chip) * Q
-            fs[2 * chip + m * Q // S, m * Q % S:m * Q % S + Q] = shares[base:base + Q].astype(BF)
+    for i in range(3, Z):
+        dense_act(in_order(i))
+    dense_down(0)
+    answer(DENSE, fs, fr, r_one.at[5], 0, 1)
     fr[me] = fs[me]
-    got = ep_send(3, lambda to: fs.at[to], fr.at[me])
-    arrive(got_e)
+    for i in range(1, Z):
+        dz = in_order(i)
+        dense_down(dz)
+        for dc in range(2):
+            answer(DENSE, fs, fr, r_one.at[5], Z - dz, dc)
+    arrive(er.at[0:T - 1], r_e.at[1])
+    arrive(er.at[0, 0:E - 1], r_e.at[0])
     total = er[0].astype(F32)
     for k in range(1, T):
         total = total + er[k].astype(F32)
     outs = total.reshape(N, DS).astype(BF)
     final = rbuf[mt] + dot(mix_hi, outs) + dot(mix_lo, outs)
-    arrive(got)
+    arrive(fr.at[0:E - 1], r_one.at[5])
     dense = fr[0].astype(F32)
     for j in range(1, E):
         dense = dense + fr[j].astype(F32)
     out[...] = final + blend * dense
-    for k in range(2, E):
-        piece(k // 2, k % 2).wait_send()
-    for c in sends:
-        c.wait_send()
+    keeps[0].start()
+    leave(xs.at[0:E - 1], NORM)
+    leave(rkr.at[0:E - 1], RANK)
+    leave(ps.at[0:E - 1], MAPS)
+    leave(pg.at[0:E - 1], GATE)
+    leave(mr.at[0:T - 1], MIXED)
+    leave(mmr.at[0:T - 1], GROUP)
+    leave(hbuf.at[0, 0:E - 1], HID)
+    leave(cs.at[0:T - 1, 0:E - 1], PICK)
+    leave(dps.at[:, 0:T - 1], PART)
+    leave(dab.at[0:T - 1], ACT)
+    leave(es.at[0:T - 1], FAR)
+    leave(es.at[0, 0:E - 1], NEAR)
+    leave(fs.at[0:E - 1], DENSE)
+    for c in keeps:
+        c.wait()
 
 
 def finish(out, rec, inner, access, out_o, rec_o, inner_o, access_o, sem):
@@ -561,7 +550,7 @@
     PW = M + LANES + C
     CAP = max(1, 2 * TOP * S // E)
     N = E * CAP
-    vmem = pl.BlockSpec(memory_space=pltpu.VMEM)
+    anywhere = pl.BlockSpec(memory_space=pl.ANY)
     hbm = pl.BlockSpec(memory_space=pltpu.HBM)
     V = pltpu.VMEM
     DMA = pltpu.SemaphoreType.DMA
@@ -585,8 +574,9 @@
         name="decode_step",
         out_shape=held,
         in_specs=[hbm] * 27,
-        out_specs=(vmem,) * 4,
+        out_specs=(anywhere,) * 4,
         scratch_shapes=[
+            V((S, DS), F32), V((S, C, STATE), F32), V((3, S, C), BF), V((S, 3, 2, GS), BF),
             V((S, D), BF), V((1, D), F32), V((HEADS, DC), BF), V((1, HEADS), F32), V((1, HEADS), F32),
             V((1, HEADS), F32), V((4, C), BF), V((2, 4, STATE), BF), V((3, S, C), BF), V((S, 3, 2, STATE), BF),
             V((1, C), F32), V((1, D), F32), V((TOP, S), jnp.int32), V((TOP, S), F32), V((D // LANES, LANES), BF),
@@ -602,8 +592,8 @@
             V((Z, T, 2, Q, U), BF), V((T, Z, 2, Q, U), BF), V((T, Z, Q, U), BF),
             V((T, E, CAP, DS), BF), V((T, E, CAP, DS), BF),
             V((E, S, DS), BF), V((E, S, DS), BF),
-            DMA((16,)), DMA((12,)), DMA((5, E)), DMA((5, E)), DMA((4, T)), DMA((4, T)),
-            DMA((E,)), DMA((E,)), DMA((T, E)), DMA((T, E)), DMA((T, E)), DMA((T, E)), DMA((T, Z)), DMA((T, Z)),
+            DMA((4,)), DMA((16,)), DMA((12,)), DMA((13,)), DMA((6,)), DMA((Z,)), DMA((E,)), DMA((T,)),
+            DMA((Z,)), DMA((Z,)), DMA((2,)),
         ],
         compiler_params=pltpu.CompilerParams(
             collective_id=0, has_side_effects=True, vmem_limit_bytes=40 * 1024 * 1024
@@ -613,7 +603,7 @@
         finish,
         name="store_results",
         out_shape=shapes,
-        in_specs=[vmem] * 4,
+        in_specs=[anywhere] * 4,
         out_specs=(hbm,) * 4,
         scratch_shapes=[DMA((8,))],
     )(*[pltpu.with_memory_space_constraint(x, pltpu.VMEM) for x in results])

time: 47.4 us -> 43.9 us (0.926)
  Pallas kernels: 46.6 us -> 43.1 us
    pallas_call x1, Pallas kernels: 45.2 us -> 41.7 us  [local(): pl.pallas_call(functools.partial(kernel, E, T, CAP), name='decode_step',...]
where the time goes in v3:
time: 43.9 us; the launch traced here: 43.7 us
  Pallas kernels  43.1 us (98%)
  between operations  0.65 us (1%)
    pallas_call x1, Pallas kernels, local(): pl.pallas_call(functools.partial(kernel, E, T, CAP), name='decode_step',...  41.7 us
    pallas_call x1, Pallas kernels, local(): pl.pallas_call(finish, name='store_results', out_shape=shapes, in_specs=[...  1.42 us

profile of v3, /device:TPU:0, one launch (start us, length us, event | category | flops | bytes accessed | tf_op | source)
XLA Modules:
  0.0 43.7 jit_solution(12580344757585679239)
XLA Ops:
  0.6 41.7 %decode_step.1 = (f32[16,512]{1,0:T(8,128)S(1)}, f32[16,256,128]{2,1,0:T(8,128)S(1)}, bf16[3,16,256]{2,1,0:T(8,128)(2,1)S(1)}, bf16[16,3,2,512]{3,2,1,0:T(2,128)(2,1)S(1)}) custom-call(bf16[16,2048]{1,0:T(8,128)(2,1)} %tokens_h.1, f32[1,2048]{1,0:T(1,128)} %bitcast.25, bf16[16,256]{1,0:T(8,128)(2,1)} %bitcast.26, f32[1,16]{1,0:T(1,128)} %bitcast.32, ...), custom_call_target="tpu_custom_call" | custom-call | tf_op jit(solution)/shard_map/decode_step/pallas_call | solution.py:572
  42.3 1.4 %store_results.1 = (f32[16,512]{1,0:T(8,128)}, f32[16,256,128]{2,1,0:T(8,128)}, bf16[3,16,256]{2,1,0:T(8,128)(2,1)}, bf16[16,3,2,512]{3,2,1,0:T(2,128)(2,1)}) custom-call(f32[16,512]{1,0:T(8,128)S(1)} %get-tuple-element.12.out, f32[16,256,128]{2,1,0:T(8,128)S(1)} %get-tuple-element.13.rec, bf16[3,16,256]{2,1,0:T(8,128)(2,1)S(1)} %get-tuple-element.14.inner, ...), custom_call_target="tpu_custom_call" | custom-call | tf_op jit(solution)/shard_map/store_results/pallas_call | solution.py:602

commit v4 on v3

--- a/solution.py
+++ b/solution.py
@@ -41,7 +41,7 @@
     tokens, mix_gain, step_weight, step_bias, decay_log, skip_scale, inner_taps, access_taps,
     inner_past, access_past, head_gain, moe_gain, ids, scores, blend_vector,
     gw, iw, ww, rw, rec, mw, eg, eu, ed, dg, du, dd,
-    xs, xr, rk, rkr, ps, pr, pg, pgr, rcat, ms, mr, mm, mmr, rbuf, hbuf, sel, cs, cr, gacc, uacc, actb, dps, dpr, dab, es, er, fs, fr,
+    xs, xr, rk, rkr, ps, pr, pg, pgr, rcat, ms, mr, mm, mmr, sc, scr, scales, hbuf, sel, cs, cr, gacc, uacc, actb, dps, dpr, dab, es, er, fs, fr,
     keep_sem, small_sem, load_sem, sent, r_one, r_n, r_h, r_c, r_d, r_a, r_e,
 ):
     me = lax.axis_index("ep")
@@ -55,14 +55,6 @@
     N = E * CAP
     M = 2 * STATE
     group = mt * (HEADS // T) // (HEADS // GROUPS)
-
-    barrier = pltpu.get_barrier_semaphore()
-    for k in range(1, E):
-        pl.semaphore_signal(barrier, inc=1, device_id={"ep": lax.rem(me + k, E)},
-                            device_id_type=pl.DeviceIdType.MESH)
-    for k in range(1, T):
-        pl.semaphore_signal(barrier, inc=1, device_id={"tp": lax.rem(mt + k, T)},
-                            device_id_type=pl.DeviceIdType.MESH)
 
     cols = pl.ds(pl.multiple_of(group * STATE, STATE), STATE)
     small = [
@@ -79,7 +71,17 @@
         (dd_w, dd), (ed_w, ed),
     ]
     loads = [pltpu.make_async_copy(a, b, load_sem.at[i]) for i, (a, b) in enumerate(pairs)]
-    for c in smalls + loads[:4]:
+    for c in smalls[:3]:
+        c.start()
+    barrier = pltpu.get_barrier_semaphore()
+    for k in range(1, E):
+        pl.semaphore_signal(barrier, inc=1, device_id={"ep": lax.rem(me + k, E)},
+                            device_id_type=pl.DeviceIdType.MESH)
+    for k in range(1, T):
+        pl.semaphore_signal(barrier, inc=1, device_id={"tp": lax.rem(mt + k, T)},
+                            device_id_type=pl.DeviceIdType.MESH)
+
+    for c in smalls[3:] + loads[:4]:
         c.start()
 
     Z = E // 2
@@ -103,7 +105,7 @@
         pltpu.make_async_copy(a, b, keep_sem.at[i])
         for i, (a, b) in enumerate([(out, out_k), (nrec, nrec_k), (inner_new, inner_k), (access_new, access_k)])
     ]
-    NORM, RANK, MAPS, GATE, MIXED, GROUP, HID, PICK, PART, ACT, FAR, NEAR, DENSE = range(13)
+    NORM, RANK, MAPS, GATE, MIXED, GROUP, HID, PICK, PART, ACT, FAR, NEAR, DENSE, REST, SCALE = range(15)
 
     def copy(src, dst, kind, recv, device):
         return pltpu.make_async_remote_copy(
@@ -147,18 +149,18 @@
     tok = tokens[...].astype(F32)
     scale = lax.rsqrt(jnp.mean(tok * tok, axis=-1, keepdims=True) + EPS)
     normed = (tok * scale * mix_gain[...]).astype(BF)
+    for j in range(E):
+        xs[j] = normed[:, j * DC:(j + 1) * DC]
+    xr[me] = xs[me]
+    pl.semaphore_wait(barrier, (E - 1) + (T - 1))
+    ep_send(NORM, lambda to: xs.at[to], xr.at[me], lambda dz: r_n.at[dz])
     names = ids[...].astype(F32)
     name_a, name_b = column(names[0:1]), column(names[1:2])
     named = jnp.where((lane_f == name_a) | (lane_f == name_b), 1.0, 0.0)
     before = dot(earlier, named)
     rank = jnp.where(named > 0.0, before, -1.0)
-    for j in range(E):
-        xs[j] = normed[:, j * DC:(j + 1) * DC]
-    xr[me] = xs[me]
     rk[...] = rank.astype(BF)
     rkr[me] = rk[...]
-    pl.semaphore_wait(barrier, (E - 1) + (T - 1))
-    ep_send(NORM, lambda to: xs.at[to], xr.at[me], lambda dz: r_n.at[dz])
     ep_send(RANK, lambda to: rk, rkr.at[me], lambda dz: r_one.at[0])
     for c in loads[4:6]:
         c.start()
@@ -282,21 +284,20 @@
     read_c = silu(past_r + maps_f[:, STATE:M] * tap_rows[3][1:2])
     read_hi = read_c.astype(BF).astype(F32)
     read_lo = read_c - read_hi
-    spare = LANES - 2 * S
-    upper = jnp.concatenate([read_hi, read_lo, jnp.zeros((spare, STATE), F32)], axis=0)
-    lower = jnp.concatenate([read_hi, jnp.zeros((spare + S, STATE), F32)], axis=0)
-    reader = jnp.concatenate([jnp.transpose(upper), jnp.transpose(lower)], axis=0).astype(BF)
+    reader = jnp.concatenate([
+        jnp.concatenate([read_hi, read_hi], axis=1),
+        jnp.concatenate([read_lo, jnp.zeros((S, STATE), F32)], axis=1)], axis=0).astype(BF)
     step_x = step_raw + step_bias[...]
     step = jnp.maximum(step_x, 0.0) + jnp.log1p(jnp.exp(-jnp.abs(step_x)))
     decay = expand(jnp.exp(-step * rate))
     push = expand(step) * inner
     both = jnp.sum(write_c * read_c, axis=-1, keepdims=True)
-    seq_lane = lax.rem(lax.broadcasted_iota(jnp.int32, (C, LANES), 1), S)
-    read_t = jnp.zeros((C, LANES), F32)
+    seq_row = lax.rem(lax.broadcasted_iota(jnp.int32, (2 * S, C), 0), S)
+    recalls = jnp.zeros((2 * S, C), F32)
     for t in range(S):
-        read_t = jnp.where(seq_lane == t, dot(rcat[t], reader), read_t)
-    read_rows = jnp.transpose(read_t)
-    recalled = read_rows[0:S] + read_rows[S:2 * S]
+        every = lax.dot_general(reader, rcat[t], (((1,), (1,)), ((), ())), preferred_element_type=F32)
+        recalls = jnp.where(seq_row == t, every, recalls)
+    recalled = recalls[0:S] + recalls[S:2 * S]
     readout = decay * recalled + push * both + skip * inner
     arrive(pgr.at[0:E - 1], r_one.at[2])
     gate_sum = pgr[0].astype(F32)
@@ -312,9 +313,16 @@
     head_out = (gated * norm * head_gain[...]).astype(BF)
     loads[5].wait()
     for j in range(T):
-        ms[:, j * DS:(j + 1) * DS] = dot(head_out, mw[:, j * DS:(j + 1) * DS]).astype(BF)
+        ms[j] = dot(head_out, mw[:, j * DS:(j + 1) * DS]).astype(BF)
+    for o in by_reach:
+        to = across(o)
+        launch(ms.at[to], mr.at[mt, to], MIXED, r_one.at[3], {"tp": to})
+    for o in by_reach:
+        for other in shifts:
+            if other != o:
+                q = across(other)
+                launch(ms.at[q], mr.at[mt, q], REST, r_one.at[6], {"tp": across(o)})
     mr[mt] = ms[...]
-    tp_send(MIXED, ms, mr.at[mt], r_one.at[3])
     mmr[mt] = mm[...]
     tp_send(GROUP, mm, mmr.at[mt], r_one.at[4])
 
@@ -325,22 +333,31 @@
     keeps[1].start()
     keeps[2].start()
 
-    arrive(mr.at[0:T - 1], r_one.at[3])
-    mixed = mr[0].astype(F32)
-    for j in range(1, T):
-        mixed = mixed + mr[j].astype(F32)
-    resid = tok + mixed.astype(BF).astype(F32)
-    scale = lax.rsqrt(jnp.mean(resid * resid, axis=-1, keepdims=True) + EPS)
-    hidden = (resid * scale * moe_gain[...]).astype(BF)
-    for q in range(T):
-        rbuf[q] = resid[:, q * DS:(q + 1) * DS]
-        hbuf[q, me] = hidden[:, q * DS:(q + 1) * DS]
-
+    arrive(mr.at[0:T - 1, 0], r_one.at[3])
+    mine = pl.ds(pl.multiple_of(mt * DS, DS), DS)
+
+    def total_of(q):
+        mixed = mr[0, q].astype(F32)
+        for j in range(1, T):
+            mixed = mixed + mr[j, q].astype(F32)
+        return mixed.astype(BF).astype(F32)
+
+    resid_own = tokens[:, mine].astype(F32) + total_of(mt)
+    hbuf[mt, me] = (resid_own * moe_gain[:, mine]).astype(BF)
     twin = chip_at(0, 1)
     for i in range(1, Z):
         dz = in_order(i)
         launch(hbuf.at[mt, me], hbuf.at[mt, me], HID, r_h.at[2 * dz], {"ep": chip_at(dz, 0)})
     launch(hbuf.at[mt, me], hbuf.at[mt, me], HID, r_h.at[1], {"ep": twin})
+
+    arrive(mr.at[0:T - 1, 0:T - 1], r_one.at[6])
+    resid = tok + jnp.concatenate([total_of(q) for q in range(T)], axis=1)
+    scale = lax.rsqrt(jnp.mean(resid * resid, axis=-1, keepdims=True) + EPS)
+    hidden = (resid * scale * moe_gain[...]).astype(BF)
+    scale_hi = scale.astype(BF).astype(F32)
+    sc[...] = jnp.where(lane < LANES // 2, scale_hi, scale - scale_hi).astype(BF)
+    scr[me] = sc[...]
+    ep_send(SCALE, lambda to: sc, scr.at[me], lambda dz: r_one.at[7])
     for q in range(T):
         chosen_q = dot(picker, hidden[:, q * DS:(q + 1) * DS])
         for e in range(E):
@@ -401,7 +418,8 @@
         dsum = dpr[0, chip].astype(F32)
         for j in range(1, T):
             dsum = dsum + dpr[j, chip].astype(F32)
-        dab[mt, chip] = (silu(dsum[0]) * dsum[1]).astype(BF)
+        by = scales[chip, mt][:, 0:1]
+        dab[mt, chip] = (silu(dsum[0] * by) * (dsum[1] * by)).astype(BF)
         for o in by_reach:
             launch(dab.at[mt, chip], dab.at[mt, chip], ACT, r_a.at[dz], {"tp": across(o)})
 
@@ -412,12 +430,14 @@
         acts = dab[:, chip].astype(F32).reshape(2 * S, U).astype(BF)
         fs[pair] = dot(acts, dd[...]).astype(BF).reshape(2, S, DS)
 
-    def expert_part(picked, q, first, last):
+    def expert_part(picked, q, first, last, factor=None):
         rows_q = pl.ds(pl.multiple_of(q * DS, DS), DS)
         for n in range(FFL // tile):
             at = slice(n * tile, (n + 1) * tile)
             g = dot(picked, eg[rows_q, at])
             u = dot(picked, eu[rows_q, at])
+            if factor is not None:
+                g, u = g * factor, u * factor
             if not first:
                 g = g + gacc[:, at]
                 u = u + uacc[:, at]
@@ -442,8 +462,13 @@
     for c in loads[8:10]:
         c.wait()
     own = dot(sel[...], hbuf[mt].reshape(E * S, DS)).astype(BF)
+    arrive(scr.at[0:E - 1], r_one.at[7])
+    halves = scr[...].reshape(E * S, LANES)
+    picked_scale = jnp.sum(dot(sel[...], halves), axis=-1, keepdims=True) * (2.0 / LANES)
+    every_scale = jnp.sum(halves.astype(F32), axis=-1, keepdims=True) * (2.0 / LANES)
+    scales[...] = jnp.broadcast_to(every_scale, (E * S, LANES)).reshape(Z, T, Q, LANES)
     dense_act(0)
-    expert_part(own, mt, True, T == 1)
+    expert_part(own, mt, True, T == 1, picked_scale)
     for n, o in enumerate(by_reach):
         q = across(o)
         arrive(cr.at[q, 0:E - 1], r_c.at[shifts.index(o)])
@@ -473,8 +498,10 @@
                         {"ep": owner, "tp": to})
         if o == by_reach[0]:
             dense_act(in_order(2))
+        if o == by_reach[2]:
+            dense_act(in_order(3))
     loads[10].wait()
-    for i in range(3, Z):
+    for i in range(4, Z):
         dense_act(in_order(i))
     dense_down(0)
     answer(DENSE, fs, fr, r_one.at[5], 0, 1)
@@ -490,7 +517,7 @@
     for k in range(1, T):
         total = total + er[k].astype(F32)
     outs = total.reshape(N, DS).astype(BF)
-    final = rbuf[mt] + dot(mix_hi, outs) + dot(mix_lo, outs)
+    final = resid_own + dot(mix_hi, outs) + dot(mix_lo, outs)
     arrive(fr.at[0:E - 1], r_one.at[5])
     dense = fr[0].astype(F32)
     for j in range(1, E):
@@ -501,7 +528,9 @@
     leave(rkr.at[0:E - 1], RANK)
     leave(ps.at[0:E - 1], MAPS)
     leave(pg.at[0:E - 1], GATE)
-    leave(mr.at[0:T - 1], MIXED)
+    leave(mr.at[0:T - 1, 0], MIXED)
+    leave(mr.at[0:T - 1, 0:T - 1], REST)
+    leave(scr.at[0:E - 1], SCALE)
     leave(mmr.at[0:T - 1], GROUP)
     leave(hbuf.at[0, 0:E - 1], HID)
     leave(cs.at[0:T - 1, 0:E - 1], PICK)
@@ -586,13 +615,13 @@
             V((DS, U), BF), V((DS, U), BF), V((U, DS), BF),
             V((E, S, DC), BF), V((E, S, DC), BF), V((S, LANES), BF), V((E, S, LANES), BF), V((E, S, PW), BF), V((E, S, PW), BF),
             V((E, S, C), BF), V((E, S, C), BF), V((S, C, M), BF),
-            V((S, D), BF), V((T, S, D), BF), V((S, M), BF), V((T, S, M), BF),
-            V((T, S, DS), F32), V((T, E, S, DS), BF),
+            V((T, S, DS), BF), V((T, T, S, DS), BF), V((S, M), BF), V((T, S, M), BF),
+            V((S, LANES), BF), V((E, S, LANES), BF), V((Z, T, Q, LANES), F32), V((T, E, S, DS), BF),
             V((N, rows), BF), V((T, E, CAP, DS), BF), V((T, E, CAP, DS), BF), V((N, FFL), F32), V((N, FFL), F32), V((N, FFL), BF),
             V((Z, T, 2, Q, U), BF), V((T, Z, 2, Q, U), BF), V((T, Z, Q, U), BF),
             V((T, E, CAP, DS), BF), V((T, E, CAP, DS), BF),
             V((E, S, DS), BF), V((E, S, DS), BF),
-            DMA((4,)), DMA((16,)), DMA((12,)), DMA((13,)), DMA((6,)), DMA((Z,)), DMA((E,)), DMA((T,)),
+            DMA((4,)), DMA((16,)), DMA((12,)), DMA((15,)), DMA((8,)), DMA((Z,)), DMA((E,)), DMA((T,)),
             DMA((Z,)), DMA((Z,)), DMA((2,)),
         ],
         compiler_params=pltpu.CompilerParams(

time: 43.9 us -> 42.7 us (0.973)
  Pallas kernels: 43.1 us -> 41.9 us
    pallas_call x1, Pallas kernels: 41.7 us -> 40.4 us  [local(): pl.pallas_call(functools.partial(kernel, E, T, CAP), name='decode_step',...]
where the time goes in v4:
time: 42.7 us; the launch traced here: 42.5 us
  Pallas kernels  41.9 us (98%)
  between operations  0.65 us (2%)
    pallas_call x1, Pallas kernels, local(): pl.pallas_call(functools.partial(kernel, E, T, CAP), name='decode_step',...  40.4 us
    pallas_call x1, Pallas kernels, local(): pl.pallas_call(finish, name='store_results', out_shape=shapes, in_specs=[...  1.42 us

profile of v4, /device:TPU:0, one launch (start us, length us, event | category | flops | bytes accessed | tf_op | source)
XLA Modules:
  0.0 42.5 jit_solution(11263805009467848082)
XLA Ops:
  0.6 40.4 %decode_step.1 = (f32[16,512]{1,0:T(8,128)S(1)}, f32[16,256,128]{2,1,0:T(8,128)S(1)}, bf16[3,16,256]{2,1,0:T(8,128)(2,1)S(1)}, bf16[16,3,2,512]{3,2,1,0:T(2,128)(2,1)S(1)}) custom-call(bf16[16,2048]{1,0:T(8,128)(2,1)} %tokens_h.1, f32[1,2048]{1,0:T(1,128)} %bitcast.25, bf16[16,256]{1,0:T(8,128)(2,1)} %bitcast.26, f32[1,16]{1,0:T(1,128)} %bitcast.32, ...), custom_call_target="tpu_custom_call" | custom-call | tf_op jit(solution)/shard_map/decode_step/pallas_call | solution.py:601
  41.1 1.4 %store_results.1 = (f32[16,512]{1,0:T(8,128)}, f32[16,256,128]{2,1,0:T(8,128)}, bf16[3,16,256]{2,1,0:T(8,128)(2,1)}, bf16[16,3,2,512]{3,2,1,0:T(2,128)(2,1)}) custom-call(f32[16,512]{1,0:T(8,128)S(1)} %get-tuple-element.12.out, f32[16,256,128]{2,1,0:T(8,128)S(1)} %get-tuple-element.13.rec, bf16[3,16,256]{2,1,0:T(8,128)(2,1)S(1)} %get-tuple-element.14.inner, ...), custom_call_target="tpu_custom_call" | custom-call | tf_op jit(solution)/shard_map/store_results/pallas_call | solution.py:631

commit v5 on v4

--- a/solution.py
+++ b/solution.py
@@ -42,7 +42,7 @@
     inner_past, access_past, head_gain, moe_gain, ids, scores, blend_vector,
     gw, iw, ww, rw, rec, mw, eg, eu, ed, dg, du, dd,
     xs, xr, rk, rkr, ps, pr, pg, pgr, rcat, ms, mr, mm, mmr, sc, scr, scales, hbuf, sel, cs, cr, gacc, uacc, actb, dps, dpr, dab, es, er, fs, fr,
-    keep_sem, small_sem, load_sem, sent, r_one, r_n, r_h, r_c, r_d, r_a, r_e,
+    keep_sem, small_sem, load_sem, sent, r_one, r_n, r_m, r_h, r_c, r_d, r_a, r_e,
 ):
     me = lax.axis_index("ep")
     mt = lax.axis_index("tp")
@@ -212,6 +212,9 @@
         ps[pair, :, M:G] = jnp.concatenate(
             [step_hi, step_lo, jnp.zeros((2 * S, LANES - 2 * HEADS), BF)], axis=1).reshape(2, S, LANES)
         ps[pair, :, G:G + C] = dot(rows, iw[...]).astype(BF).reshape(2, S, C)
+        return pair, rows
+
+    def project_gate(pair, rows):
         pg[pair] = dot(rows, gw[...]).astype(BF).reshape(2, S, C)
 
     def answer(kind, src, dst, recv, back, dc):
@@ -219,17 +222,19 @@
         launch(src.at[to], dst.at[me], kind, recv, {"ep": to})
 
     arrive(xr.at[0], r_n.at[0])
-    project(0)
-    answer(MAPS, ps, pr, r_one.at[1], 0, 1)
+    work = project(0)
+    answer(MAPS, ps, pr, r_m.at[0], 0, 1)
+    project_gate(*work)
     answer(GATE, pg, pgr, r_one.at[2], 0, 1)
     pr[me] = ps[me]
     pgr[me] = pg[me]
     for i in range(1, Z):
         dz = in_order(i)
         arrive(xr.at[0:2], r_n.at[dz])
-        project(dz)
+        work = project(dz)
         for dc in range(2):
-            answer(MAPS, ps, pr, r_one.at[1], Z - dz, dc)
+            answer(MAPS, ps, pr, r_m.at[Z - dz], Z - dz, dc)
+        project_gate(*work)
         for dc in range(2):
             answer(GATE, pg, pgr, r_one.at[2], Z - dz, dc)
     for c in loads[6:]:
@@ -265,14 +270,15 @@
     @pl.loop(0, S)
     def _(t):
         value = rec[t]
-        high = value.astype(BF)
-        rcat[t, :, 0:STATE] = high
-        rcat[t, :, STATE:M] = (value - high.astype(F32)).astype(BF)
-
-    arrive(pr.at[0:E - 1], r_one.at[1])
-    proj = pr[0].astype(F32)
-    for j in range(1, E):
-        proj = proj + pr[j].astype(F32)
+        rcat[t] = value.astype(BF)
+
+    arrive(pr.at[0], r_m.at[0])
+    proj = pr[me].astype(F32) + pr[chip_at(0, 1)].astype(F32)
+    for i in range(1, Z):
+        dz = in_order(i)
+        arrive(pr.at[0:2], r_m.at[dz])
+        proj = proj + pr[chip_at(Z - dz, 0)].astype(F32)
+        proj = proj + pr[chip_at(Z - dz, 1)].astype(F32)
     maps = proj[:, 0:M].astype(BF)
     step_raw = proj[:, M:M + HEADS] + proj[:, M + HEADS:M + 2 * HEADS]
     inner_part = proj[:, G:G + C].astype(BF)
@@ -284,9 +290,7 @@
     read_c = silu(past_r + maps_f[:, STATE:M] * tap_rows[3][1:2])
     read_hi = read_c.astype(BF).astype(F32)
     read_lo = read_c - read_hi
-    reader = jnp.concatenate([
-        jnp.concatenate([read_hi, read_hi], axis=1),
-        jnp.concatenate([read_lo, jnp.zeros((S, STATE), F32)], axis=1)], axis=0).astype(BF)
+    reader = jnp.concatenate([read_hi, read_lo], axis=0).astype(BF)
     step_x = step_raw + step_bias[...]
     step = jnp.maximum(step_x, 0.0) + jnp.log1p(jnp.exp(-jnp.abs(step_x)))
     decay = expand(jnp.exp(-step * rate))
@@ -312,11 +316,12 @@
         norm = jnp.where(here, lax.rsqrt(mean + EPS), norm)
     head_out = (gated * norm * head_gain[...]).astype(BF)
     loads[5].wait()
-    for j in range(T):
-        ms[j] = dot(head_out, mw[:, j * DS:(j + 1) * DS]).astype(BF)
-    for o in by_reach:
+    for o in by_reach + shifts[:1]:
         to = across(o)
-        launch(ms.at[to], mr.at[mt, to], MIXED, r_one.at[3], {"tp": to})
+        wide_to = pl.ds(pl.multiple_of(to * DS, DS), DS)
+        ms[to] = dot(head_out, mw[:, wide_to]).astype(BF)
+        if o != shifts[0]:
+            launch(ms.at[to], mr.at[mt, to], MIXED, r_one.at[3], {"tp": to})
     for o in by_reach:
         for other in shifts:
             if other != o:
@@ -350,6 +355,24 @@
         launch(hbuf.at[mt, me], hbuf.at[mt, me], HID, r_h.at[2 * dz], {"ep": chip_at(dz, 0)})
     launch(hbuf.at[mt, me], hbuf.at[mt, me], HID, r_h.at[1], {"ep": twin})
 
+    Q = 2 * S // T
+
+    def dense_part(dz):
+        chip = lax.rem(z + Z - dz, Z)
+        here = hbuf[mt, pl.ds(2 * chip, 2)].reshape(2 * S, DS)
+        for w, weight in enumerate((dg, du)):
+            part = dot(here, weight[...])
+            for m in range(T):
+                dps[chip, m, w] = part[m * Q:(m + 1) * Q].astype(BF)
+        for o in by_reach:
+            to = across(o)
+            launch(dps.at[chip, to], dpr.at[mt, chip], PART, r_d.at[dz], {"tp": to})
+        dpr[mt, chip] = dps[chip, mt]
+
+    for c in loads[6:8]:
+        c.wait()
+    arrive(hbuf.at[mt, twin], r_h.at[1])
+    dense_part(0)
     arrive(mr.at[0:T - 1, 0:T - 1], r_one.at[6])
     resid = tok + jnp.concatenate([total_of(q) for q in range(T)], axis=1)
     scale = lax.rsqrt(jnp.mean(resid * resid, axis=-1, keepdims=True) + EPS)
@@ -372,22 +395,6 @@
                     to = chip_at(dz, dc)
                     launch(cs.at[q, to], cr.at[q, me], PICK, r_c.at[n], {"ep": to})
 
-    scorer = blend_vector[...].astype(F32)
-    blend = jnp.zeros((S, LANES), F32)
-    for j in range(D // LANES):
-        blend = blend + hidden[:, j * LANES:(j + 1) * LANES].astype(F32) * scorer[j:j + 1]
-    blend = jnp.sum(blend, axis=-1, keepdims=True)
-    blend = 1.0 / (1.0 + jnp.exp(-blend))
-
-    arrive(mmr.at[0:T - 1], r_one.at[4])
-    smalls[15].wait()
-    owners = [mmr[g * max(1, T // GROUPS)].astype(F32) for g in range(GROUPS)]
-    for s in range(S):
-        for g in range(GROUPS):
-            pair = jnp.concatenate([owners[g][s:s + 1, 0:STATE], owners[g][s:s + 1, STATE:M]], axis=0)
-            access_new[s, 2, :, g * STATE:(g + 1) * STATE] = pair.astype(BF)
-    keeps[3].start()
-
     def relay(i):
         dz = in_order(i)
         block = hbuf.at[mt, chip_at(Z - dz, 0)]
@@ -397,20 +404,6 @@
     def passed(i):
         dz = in_order(i)
         arrive(hbuf.at[mt, chip_at(Z - dz, 1)], r_h.at[2 * dz + 1])
-
-    Q = 2 * S // T
-
-    def dense_part(dz):
-        chip = lax.rem(z + Z - dz, Z)
-        here = hbuf[mt, pl.ds(2 * chip, 2)].reshape(2 * S, DS)
-        for w, weight in enumerate((dg, du)):
-            part = dot(here, weight[...])
-            for m in range(T):
-                dps[chip, m, w] = part[m * Q:(m + 1) * Q].astype(BF)
-        for o in by_reach:
-            to = across(o)
-            launch(dps.at[chip, to], dpr.at[mt, chip], PART, r_d.at[dz], {"tp": to})
-        dpr[mt, chip] = dps[chip, mt]
 
     def dense_act(dz):
         chip = lax.rem(z + Z - dz, Z)
@@ -448,10 +441,6 @@
                 uacc[:, at] = u
 
     tile = tile_of(FFL)
-    for c in loads[6:8]:
-        c.wait()
-    arrive(hbuf.at[mt, twin], r_h.at[1])
-    dense_part(0)
     for i in range(1, Z):
         relay(i)
         if i > 1:
@@ -479,7 +468,7 @@
 
     loads[11].wait()
     dtile = tile_of(DS)
-    for o in by_reach + shifts[:1]:
+    for n_o, o in enumerate(by_reach + shifts[:1]):
         to, k = across(o), shifts.index(o)
         for n in range(DS // dtile):
             at = pl.ds(pl.multiple_of(to * DS + n * dtile, dtile), dtile)
@@ -496,13 +485,29 @@
                     launch(
                         es.at[k, owner], er.at[k, me], FAR if k > 0 else NEAR, r_e.at[min(k, 1)],
                         {"ep": owner, "tp": to})
-        if o == by_reach[0]:
+        if n_o == 0:
             dense_act(in_order(2))
-        if o == by_reach[2]:
+        if n_o == 2:
             dense_act(in_order(3))
     loads[10].wait()
     for i in range(4, Z):
         dense_act(in_order(i))
+    scorer = blend_vector[...].astype(F32)
+    blend = jnp.zeros((S, LANES), F32)
+    for j in range(D // LANES):
+        blend = blend + hidden[:, j * LANES:(j + 1) * LANES].astype(F32) * scorer[j:j + 1]
+    blend = jnp.sum(blend, axis=-1, keepdims=True)
+    blend = 1.0 / (1.0 + jnp.exp(-blend))
+
+    arrive(mmr.at[0:T - 1], r_one.at[4])
+    smalls[15].wait()
+    owners = [mmr[g * max(1, T // GROUPS)].astype(F32) for g in range(GROUPS)]
+    for s in range(S):
+        for g in range(GROUPS):
+            pair = jnp.concatenate([owners[g][s:s + 1, 0:STATE], owners[g][s:s + 1, STATE:M]], axis=0)
+            access_new[s, 2, :, g * STATE:(g + 1) * STATE] = pair.astype(BF)
+    keeps[3].start()
+
     dense_down(0)
     answer(DENSE, fs, fr, r_one.at[5], 0, 1)
     fr[me] = fs[me]
@@ -614,14 +619,14 @@
             V((D, FFL), BF), V((D, FFL), BF), V((FFL, D), BF),
             V((DS, U), BF), V((DS, U), BF), V((U, DS), BF),
             V((E, S, DC), BF), V((E, S, DC), BF), V((S, LANES), BF), V((E, S, LANES), BF), V((E, S, PW), BF), V((E, S, PW), BF),
-            V((E, S, C), BF), V((E, S, C), BF), V((S, C, M), BF),
+            V((E, S, C), BF), V((E, S, C), BF), V((S, C, STATE), BF),
             V((T, S, DS), BF), V((T, T, S, DS), BF), V((S, M), BF), V((T, S, M), BF),
             V((S, LANES), BF), V((E, S, LANES), BF), V((Z, T, Q, LANES), F32), V((T, E, S, DS), BF),
             V((N, rows), BF), V((T, E, CAP, DS), BF), V((T, E, CAP, DS), BF), V((N, FFL), F32), V((N, FFL), F32), V((N, FFL), BF),
             V((Z, T, 2, Q, U), BF), V((T, Z, 2, Q, U), BF), V((T, Z, Q, U), BF),
             V((T, E, CAP, DS), BF), V((T, E, CAP, DS), BF),
             V((E, S, DS), BF), V((E, S, DS), BF),
-            DMA((4,)), DMA((16,)), DMA((12,)), DMA((15,)), DMA((8,)), DMA((Z,)), DMA((E,)), DMA((T,)),
+            DMA((4,)), DMA((16,)), DMA((12,)), DMA((15,)), DMA((8,)), DMA((Z,)), DMA((Z,)), DMA((E,)), DMA((T,)),
             DMA((Z,)), DMA((Z,)), DMA((2,)),
         ],
         compiler_params=pltpu.CompilerParams(

time: 42.7 us -> 42.4 us (level)
  no operation moved by 1% of the time
where the time goes in v5:
time: 42.4 us; the launch traced here: 42.2 us
  Pallas kernels  41.6 us (98%)
  between operations  0.65 us (2%)
    pallas_call x1, Pallas kernels, local(): pl.pallas_call(functools.partial(kernel, E, T, CAP), name='decode_step',...  40.2 us
    pallas_call x1, Pallas kernels, local(): pl.pallas_call(finish, name='store_results', out_shape=shapes, in_specs=[...  1.42 us

profile of v5, /device:TPU:0, one launch (start us, length us, event | category | flops | bytes accessed | tf_op | source)
XLA Modules:
  0.0 42.2 jit_solution(5710856662159472452)
XLA Ops:
  0.6 40.2 %decode_step.1 = (f32[16,512]{1,0:T(8,128)S(1)}, f32[16,256,128]{2,1,0:T(8,128)S(1)}, bf16[3,16,256]{2,1,0:T(8,128)(2,1)S(1)}, bf16[16,3,2,512]{3,2,1,0:T(2,128)(2,1)S(1)}) custom-call(bf16[16,2048]{1,0:T(8,128)(2,1)} %tokens_h.1, f32[1,2048]{1,0:T(1,128)} %bitcast.25, bf16[16,256]{1,0:T(8,128)(2,1)} %bitcast.26, f32[1,16]{1,0:T(1,128)} %bitcast.32, ...), custom_call_target="tpu_custom_call" | custom-call | tf_op jit(solution)/shard_map/decode_step/pallas_call | solution.py:606
  40.8 1.4 %store_results.1 = (f32[16,512]{1,0:T(8,128)}, f32[16,256,128]{2,1,0:T(8,128)}, bf16[3,16,256]{2,1,0:T(8,128)(2,1)}, bf16[16,3,2,512]{3,2,1,0:T(2,128)(2,1)}) custom-call(f32[16,512]{1,0:T(8,128)S(1)} %get-tuple-element.12.out, f32[16,256,128]{2,1,0:T(8,128)S(1)} %get-tuple-element.13.rec, bf16[3,16,256]{2,1,0:T(8,128)(2,1)S(1)} %get-tuple-element.14.inner, ...), custom_call_target="tpu_custom_call" | custom-call | tf_op jit(solution)/shard_map/store_results/pallas_call | solution.py:636

commit v6 on v5

--- a/solution.py
+++ b/solution.py
@@ -105,7 +105,8 @@
         pltpu.make_async_copy(a, b, keep_sem.at[i])
         for i, (a, b) in enumerate([(out, out_k), (nrec, nrec_k), (inner_new, inner_k), (access_new, access_k)])
     ]
-    NORM, RANK, MAPS, GATE, MIXED, GROUP, HID, PICK, PART, ACT, FAR, NEAR, DENSE, REST, SCALE = range(15)
+    NORM, RANK, MAPS, GATE, MIXED, GROUP, HID, PICK, PART, ACT, FAR, SCALE = range(12)
+    REST, NEAR, DENSE = MIXED, PICK, HID
 
     def copy(src, dst, kind, recv, device):
         return pltpu.make_async_remote_copy(
@@ -331,13 +332,6 @@
     mmr[mt] = mm[...]
     tp_send(GROUP, mm, mmr.at[mt], r_one.at[4])
 
-    decay_t = jnp.transpose(decay)
-    push_t = jnp.transpose(push)
-    for t in range(S):
-        nrec[t] = decay_t[:, t:t + 1] * rec[t] + push_t[:, t:t + 1] * write_c[t:t + 1]
-    keeps[1].start()
-    keeps[2].start()
-
     arrive(mr.at[0:T - 1, 0], r_one.at[3])
     mine = pl.ds(pl.multiple_of(mt * DS, DS), DS)
 
@@ -354,6 +348,13 @@
         dz = in_order(i)
         launch(hbuf.at[mt, me], hbuf.at[mt, me], HID, r_h.at[2 * dz], {"ep": chip_at(dz, 0)})
     launch(hbuf.at[mt, me], hbuf.at[mt, me], HID, r_h.at[1], {"ep": twin})
+    decay_t = jnp.transpose(decay)
+    push_t = jnp.transpose(push)
+    for t in range(S):
+        nrec[t] = decay_t[:, t:t + 1] * rec[t] + push_t[:, t:t + 1] * write_c[t:t + 1]
+    keeps[1].start()
+    keeps[2].start()
+
 
     Q = 2 * S // T
 
@@ -533,17 +534,14 @@
     leave(rkr.at[0:E - 1], RANK)
     leave(ps.at[0:E - 1], MAPS)
     leave(pg.at[0:E - 1], GATE)
-    leave(mr.at[0:T - 1, 0], MIXED)
-    leave(mr.at[0:T - 1, 0:T - 1], REST)
+    leave(mr.at[0:T - 1, 0:T], MIXED)
     leave(scr.at[0:E - 1], SCALE)
     leave(mmr.at[0:T - 1], GROUP)
-    leave(hbuf.at[0, 0:E - 1], HID)
-    leave(cs.at[0:T - 1, 0:E - 1], PICK)
+    leave(hbuf.at[0:2, 0:E - 1], HID)
+    leave(cs.at[0:T, 0:E - 1], PICK)
     leave(dps.at[:, 0:T - 1], PART)
     leave(dab.at[0:T - 1], ACT)
     leave(es.at[0:T - 1], FAR)
-    leave(es.at[0, 0:E - 1], NEAR)
-    leave(fs.at[0:E - 1], DENSE)
     for c in keeps:
         c.wait()
 
@@ -626,7 +624,7 @@
             V((Z, T, 2, Q, U), BF), V((T, Z, 2, Q, U), BF), V((T, Z, Q, U), BF),
             V((T, E, CAP, DS), BF), V((T, E, CAP, DS), BF),
             V((E, S, DS), BF), V((E, S, DS), BF),
-            DMA((4,)), DMA((16,)), DMA((12,)), DMA((15,)), DMA((8,)), DMA((Z,)), DMA((Z,)), DMA((E,)), DMA((T,)),
+            DMA((4,)), DMA((16,)), DMA((12,)), DMA((12,)), DMA((8,)), DMA((Z,)), DMA((Z,)), DMA((E,)), DMA((T,)),
             DMA((Z,)), DMA((Z,)), DMA((2,)),
         ],
         compiler_params=pltpu.CompilerParams(

time: 42.4 us -> 42.3 us (level)
  no operation moved by 1% of the time
where the time goes in v6:
time: 42.3 us; the launch traced here: 42.2 us
  Pallas kernels  41.5 us (98%)
  between operations  0.65 us (2%)
    pallas_call x1, Pallas kernels, local(): pl.pallas_call(functools.partial(kernel, E, T, CAP), name='decode_step',...  40.1 us
    pallas_call x1, Pallas kernels, local(): pl.pallas_call(finish, name='store_results', out_shape=shapes, in_specs=[...  1.42 us

profile of v6, /device:TPU:0, one launch (start us, length us, event | category | flops | bytes accessed | tf_op | source)
XLA Modules:
  0.0 42.2 jit_solution(7060702358635245159)
XLA Ops:
  0.6 40.1 %decode_step.1 = (f32[16,512]{1,0:T(8,128)S(1)}, f32[16,256,128]{2,1,0:T(8,128)S(1)}, bf16[3,16,256]{2,1,0:T(8,128)(2,1)S(1)}, bf16[16,3,2,512]{3,2,1,0:T(2,128)(2,1)S(1)}) custom-call(bf16[16,2048]{1,0:T(8,128)(2,1)} %tokens_h.1, f32[1,2048]{1,0:T(1,128)} %bitcast.25, bf16[16,256]{1,0:T(8,128)(2,1)} %bitcast.26, f32[1,16]{1,0:T(1,128)} %bitcast.32, ...), custom_call_target="tpu_custom_call" | custom-call | tf_op jit(solution)/shard_map/decode_step/pallas_call | solution.py:604
  40.8 1.4 %store_results.1 = (f32[16,512]{1,0:T(8,128)}, f32[16,256,128]{2,1,0:T(8,128)}, bf16[3,16,256]{2,1,0:T(8,128)(2,1)}, bf16[16,3,2,512]{3,2,1,0:T(2,128)(2,1)}) custom-call(f32[16,512]{1,0:T(8,128)S(1)} %get-tuple-element.12.out, f32[16,256,128]{2,1,0:T(8,128)S(1)} %get-tuple-element.13.rec, bf16[3,16,256]{2,1,0:T(8,128)(2,1)S(1)} %get-tuple-element.14.inner, ...), custom_call_target="tpu_custom_call" | custom-call | tf_op jit(solution)/shard_map/store_results/pallas_call | solution.py:634
